TPU v7x, 32 devices: a whole 2x2x4 slice. The times are simulated.
32 devices in a mesh: sp: 16 (over z, y, core), tp: 2 (over x).
Axes of the slice: x: 2, y: 2, z: 4, core: 2. Of those that a mesh axis runs over, the one named last changes fastest.
Arguments:
- tokens: bfloat16 [8192, 2048], P(('sp', 'tp')), may hold values from -6 to 6
- norm_gain: float32 [2048], replicated, may hold values from 0.1 to 1.9
- query_weight: bfloat16 [2048, 1024], P(None, 'tp'), may hold values from -0.13258252 to 0.13258252
- key_weight: bfloat16 [2048, 1024], P(None, 'tp'), may hold values from -0.13258252 to 0.13258252
- value_weight: bfloat16 [2048, 1024], P(None, 'tp'), may hold values from -0.125 to 0.125
- glu_value_weight: bfloat16 [2048, 1024], P(None, 'tp'), may hold values from -0.125 to 0.125
- glu_gate_weight: bfloat16 [2048, 1024], P(None, 'tp'), may hold values from -0.125 to 0.125
- qk_gain: float32 [2, 64], replicated, may hold values from 1 to 6
- mix_lambda: float32 [8], P('tp'), may hold values from 0.3 to 0.8
- head_gain: float32 [128], replicated, may hold values from 0.1 to 1.9
- conv_kernel: float32 [31, 1024], P(None, 'tp'), may hold values from -1 to 1
- channel_gain: float32 [1024], P('tp'), may hold values from 0.1 to 1.9
- channel_shift: float32 [1024], P('tp'), may hold values from -3 to 3
- output_weight: bfloat16 [2048, 2048], replicated, may hold values from -0.125 to 0.125
Outputs:
- mixed: bfloat16 [8192, 2048], P(('sp', 'tp'))
- log_totals: float32 [2, 8, 8192], P(None, 'tp', 'sp')
All inputs are finite; a program needn't handle non-finite values.
Results may differ from a plain program's by a relative error of at most 0.035.
Values may be sent and summed in bfloat16 or wider, within the bound.
A program may use at most 128 MiB of HBM per device.

v0:
```python
import math

import jax
import jax.numpy as jnp
from jax import lax
from jax.sharding import PartitionSpec as P


def from_behind(value, axis, steps):
    count = lax.axis_size(axis)
    leading, last = (max(0, -steps), min(count, count - steps))
    return lax.ppermute(value, axis, [(source, source + steps) for source in range(leading, last)])


def rotate(values, positions):
    half = values.shape[-1] // 2
    inverse = 10000.0 ** (-jnp.arange(0, half, dtype=jnp.float32) * 2.0 / values.shape[-1])
    angles = positions[:, None] * inverse[None, :]
    cosine = jnp.cos(angles)[:, None, None, :]
    sine = jnp.sin(angles)[:, None, None, :]
    first = values[..., :half]
    second = values[..., half:]
    return jnp.concatenate(
        [first * cosine - second * sine, second * cosine + first * sine], axis=-1
    )


def prepare(raw, qk_gain, positions):
    values = raw.astype(jnp.float32)
    values = values * lax.rsqrt(jnp.mean(values * values, axis=-1, keepdims=True) + 1e-06)
    values = values * qk_gain[None, None, :, :]
    return rotate(values, positions).astype(jnp.bfloat16)


def per_device(
    tokens,
    norm_gain,
    query_weight,
    key_weight,
    value_weight,
    glu_value_weight,
    glu_gate_weight,
    qk_gain,
    mix_lambda,
    head_gain,
    conv_kernel,
    channel_gain,
    channel_shift,
    output_weight,
):
    head_size = qk_gain.shape[1]
    heads_here = mix_lambda.shape[0]
    value_size = head_gain.shape[0]
    kernel_len = conv_kernel.shape[0]
    conv_here = conv_kernel.shape[1]
    width = tokens.shape[1]
    matrices = (query_weight, key_weight, value_weight, glu_value_weight, glu_gate_weight)

    def project(piece):
        inputs = piece.astype(jnp.float32)
        normed = (
            inputs
            * lax.rsqrt(jnp.mean(inputs * inputs, axis=-1, keepdims=True) + 1e-06)
            * norm_gain
        ).astype(jnp.bfloat16)
        results = [
            jnp.dot(normed, matrix, preferred_element_type=jnp.float32).astype(jnp.bfloat16)
            for matrix in matrices
        ]
        return jnp.concatenate(results, axis=1)

    projected = project(lax.all_gather(tokens, "tp", axis=0, tiled=True))
    tok_rows = projected.shape[0]
    bounds = [0]
    for matrix in matrices:
        bounds.append(bounds[-1] + matrix.shape[1])
    queries = projected[:, bounds[0] : bounds[1]].reshape(tok_rows, heads_here, 2, head_size)
    keys = projected[:, bounds[1] : bounds[2]].reshape(tok_rows, heads_here, 2, head_size)
    values = projected[:, bounds[2] : bounds[3]].reshape(tok_rows, heads_here, value_size)
    glu_a = projected[:, bounds[3] : bounds[4]]
    glu_g = projected[:, bounds[4] : bounds[5]]
    offset = lax.axis_index("sp") * tok_rows
    query_pos = offset + jnp.arange(tok_rows, dtype=jnp.int32)
    float_pos = query_pos.astype(jnp.float32)
    rq = jnp.transpose(prepare(queries, qk_gain, float_pos), (1, 2, 0, 3))
    rk = prepare(keys, qk_gain, float_pos)
    scale = head_size ** (-0.5)
    last_query = offset + tok_rows - 1
    initial = (
        jnp.full((heads_here, 2, tok_rows), -1e30, jnp.float32),
        jnp.zeros((heads_here, 2, tok_rows), jnp.float32),
        jnp.zeros((heads_here, 2, tok_rows, value_size), jnp.float32),
    )
    carry = initial
    key_piece = lax.all_gather(rk, "sp", axis=0, tiled=True)
    value_piece = lax.all_gather(values, "sp", axis=0, tiled=True)
    count = key_piece.shape[0]
    block = math.gcd(count, 512)
    blocks = count // block
    key_blocks = key_piece.reshape(blocks, block, heads_here, 2, head_size)
    value_blocks = value_piece.reshape(blocks, block, heads_here, value_size)

    def advance(state, item):
        key_block, value_block, number = item
        key_start = number * block

        def compute(inner):
            running, totals, summed = inner
            scores = (
                jnp.einsum("hmqd,khmd->hmqk", rq, key_block, preferred_element_type=jnp.float32)
                * scale
            )
            key_pos = key_start + jnp.arange(block, dtype=jnp.int32)
            allowed = key_pos[None, :] <= query_pos[:, None]
            scores = jnp.where(allowed[None, None], scores, -1e30)
            newtop = jnp.maximum(running, jnp.max(scores, axis=-1))
            probs = jnp.where(allowed[None, None], jnp.exp(scores - newtop[..., None]), 0.0)
            factor = jnp.exp(running - newtop)
            totals = totals * factor + jnp.sum(probs, axis=-1)
            added = jnp.einsum(
                "hmqk,khd->hmqd",
                probs.astype(jnp.bfloat16),
                value_block,
                preferred_element_type=jnp.float32,
            )
            return (newtop, totals, summed * factor[..., None] + added)

        def keep(inner):
            return inner

        return (lax.cond(key_start <= last_query, compute, keep, state), None)

    carry, unused = lax.scan(
        advance, carry, (key_blocks, value_blocks, jnp.arange(blocks, dtype=jnp.int32))
    )
    running, totals, summed = carry
    heads_out = (
        summed[:, 0] / totals[:, 0, :, None]
        - mix_lambda[:, None, None] * summed[:, 1] / totals[:, 1, :, None]
    )
    heads_out = (
        heads_out
        * lax.rsqrt(jnp.mean(heads_out * heads_out, axis=-1, keepdims=True) + 1e-06)
        * head_gain
    )
    attended = jnp.transpose(heads_out.astype(jnp.bfloat16), (1, 0, 2)).reshape(
        tok_rows, heads_here * value_size
    )
    log_totals = jnp.transpose(running + jnp.log(totals), (1, 0, 2))
    gated = (glu_a.astype(jnp.float32) * jax.nn.sigmoid(glu_g.astype(jnp.float32))).astype(
        jnp.bfloat16
    )
    earlier = from_behind(gated[tok_rows - (kernel_len - 1) :], "sp", 1)
    extended = jnp.concatenate([earlier, gated], axis=0).astype(jnp.float32)
    convolved = jnp.zeros((tok_rows, conv_here), jnp.float32)
    for step in range(kernel_len):
        convolved = convolved + conv_kernel[step][None, :] * extended[step : step + tok_rows]
    plain_sum, square_sum = lax.psum(
        (jnp.sum(convolved, axis=1), jnp.sum(convolved * convolved, axis=1)), "tp"
    )
    channels = conv_here * lax.axis_size("tp")
    middle = (plain_sum / channels)[:, None]
    spread = (square_sum / channels)[:, None] - middle * middle
    conv_out = jax.nn.silu(
        (convolved - middle) * lax.rsqrt(spread + 1e-05) * channel_gain + channel_shift
    ).astype(jnp.bfloat16)
    merged = jnp.concatenate([attended, conv_out], axis=1)
    groups = lax.axis_size("tp")
    branch_width = heads_here * value_size
    weight_view = output_weight.reshape(2, groups, branch_width, width)
    moved = lax.all_to_all(merged, "tp", split_axis=0, concat_axis=1, tiled=True)
    arranged = moved.reshape(tok_rows // groups, groups, 2, branch_width)
    mixed = jnp.einsum(
        "rtcj,ctjd->rd", arranged, weight_view, preferred_element_type=jnp.float32
    ).astype(jnp.bfloat16)
    return (mixed, log_totals)


def solution(mesh):
    placed = (
        P(("sp", "tp"), None),
        P(),
        P(None, "tp"),
        P(None, "tp"),
        P(None, "tp"),
        P(None, "tp"),
        P(None, "tp"),
        P(),
        P("tp"),
        P(),
        P(None, "tp"),
        P("tp"),
        P("tp"),
        P(),
    )
    return jax.shard_map(
        per_device,
        mesh=mesh,
        in_specs=placed,
        out_specs=(P(("sp", "tp"), None), P(None, "tp", "sp")),
        check_vma=False,
    )
```

profile of v0, /device:TPU:29, one launch (start us, length us, event | category | flops | bytes accessed | tf_op | source)
XLA Modules:
  0.0 434.6 jit_solution(18231954651570132200)
XLA Ops:
  8.0 35.5 %all-gather.4.cloned.1.call-done = bf16[512,2048]{1,0:T(8,128)(2,1)} async-done(((bf16[256,2048]{1,0:T(8,128)(2,1)}), bf16[512,2048]{1,0:T(8,128)(2,1)}) %all-gather.4.cloned.1.call-update) | async-done | bytes 2097168 | tf_op jit(solution)/shard_map/all_gather | solution.py:72
  45.7 3.0 convolution_convert_fusion.2
  50.2 3.1 fusion.34
  56.6 3.9 fusion.31
  65.7 5.0 %fusion.77 = (f32[512]{0:T(512)S(1)}, f32[512]{0:T(512)S(1)}, f32[512,512]{1,0:T(8,128)S(1)}) fusion(f32[542,512]{1,0:T(8,128)S(1)} %maximum_convert_fusion, f32[512]{0:T(512)S(1)} %bitcast.147, f32[512]{0:T(512)S(1)} %bitcast.148, f32[512]{0:T(512)S(1)} %bitcast.150, f32[512]{0:T(512)S(1)} %bitcast.151, f32[512]{0:T(512)S(1)} %bitcast.152, ...), kind=kLoop, calls=%fused_computation.148 | loop fusion | flops 16776192 | bytes 33622016 | tf_op jit(solution)/shard_map/reduce_sum | solution.py:159
  70.7 4.4 %all-reduce = (f32[512]{0:T(512)S(1)}, f32[512]{0:T(512)S(1)}) all-reduce(f32[512]{0:T(512)S(1)} %get-tuple-element.182, f32[512]{0:T(512)S(1)} %get-tuple-element.181), channel_id=1, replica_groups=mesh['sp'=16,'tp'=2] {'tp'}, use_global_device_ids=true, to_apply=%region_13.14 | all-reduce | flops 1024 | bytes 8192 | tf_op jit(solution)/shard_map/psum | solution.py:158
  75.5 47.3 %all-gather.8.cloned.1.call-done = bf16[8192,4,128]{2,0,1:T(8,128)(2,1)} async-done(((bf16[512,4,128]{2,0,1:T(8,128)(2,1)}), bf16[8192,4,128]{2,0,1:T(8,128)(2,1)}) %all-gather.8.cloned.1.call-update) | async-done | bytes 8388624 | tf_op jit(solution)/shard_map/all_gather | solution.py:96
  122.8 7.6 %copy.23 = bf16[16,512,4,128]{3,1,2,0:T(8,128)(2,1)} copy(bf16[16,512,4,128]{3,1,0,2:T(8,128)(2,1)} %bitcast.123) | data formatting | bytes 16777216
  130.4 71.0 %all-gather.6.cloned.1.call-done = bf16[8192,4,2,64]{0,3,2,1:T(8,128)(2,1)} async-done(((bf16[512,4,2,64]{0,3,2,1:T(8,128)(2,1)}), bf16[8192,4,2,64]{0,3,2,1:T(8,128)(2,1)}) %all-gather.6.cloned.1.call-update) | async-done | bytes 8388624 | tf_op jit(solution)/shard_map/all_gather | solution.py:95
  201.4 7.9 %copy.51 = bf16[4,2,8,16,8,512]{5,4,2,1,0,3:T(8,128)(2,1)} copy(bf16[4,2,8,16,8,512]{5,4,3,2,1,0:T(8,128)(2,1)} %bitcast.124) | data formatting | bytes 16777216 | tf_op jit(solution)/shard_map/reshape | solution.py:100
  210.8 193.6 %while.15 = (s32[]{:T(128)}, f32[4,2,512]{2,1,0:T(2,128)S(1)}, f32[4,2,512]{2,1,0:T(2,128)S(1)}, f32[4,2,512,128]{3,2,1,0:T(8,128)}, s32[16]{0:T(128)S(1)}, /*in...) while((s32[]{:T(128)}, f32[4,2,512]{2,1,0:T(2,128)S(1)}, ...), condition=%wide.region_8.9_spmd.clone, body=%wide.region_3.8_spmd.clone.sunk | while | flops 833889280 | bytes 49034600 | solution.py:133
  212.1 10.8 %conditional.3 = ((f32[4,2,512]{2,1,0:T(2,128)S(1)}, f32[4,2,512]{2,1,0:T(2,128)S(1)}, f32[4,2,512,128]{3,2,1,0:T(8,128)})) conditional(s32[]{:T(128)} %convert_element_type.168, (f32[4,2,512]{2,1,0:T(2,128)S(1)}, f32[4,2,512]{2,1,0:T(2,128)S(1)}, f32[4,2,512,128]{3,2,1,0:T(8,128)}) %tuple.88, (s32[]{:T(128)}, s32[]{:T(128)}, ...), branch_computations={%region_4.4_spmd, %region_5.7_spmd} | conditional | flops 833889280 | bytes 49032288 | solution.py:131
  212.3 2.5 fusion.2
  217.0 4.6 %multiply_add_fusion = f32[4,2,512,128]{3,2,1,0:T(8,128)S(1)} fusion(f32[4,2,512,128]{3,2,1,0:T(8,128)S(1)} %copy-done.2, f32[4,2,512,512]{3,2,1,0:T(8,128)S(1)} %get-tuple-element.211, f32[4,2,512]{2,1,0:T(2,128)S(1)} %max.4, pred[512,512]{0,1:T(8,128)(4,1)S(1)} %broadcast_compare_fusion, f32[4,2,512]{2,1,0:T(2,128)S(1)} %bitcast.134, ...), kind=kOutput, calls=%fused_computation.8 | convolution fusion | flops 548405248 | bytes 13402624 | tf_op jit(solution)/shard_map/while/body/eval_jaxpr/cond/branch_1_fun/hmqk,khd->hmqd/dot_general | solution.py:120
  224.2 10.8 %conditional.3 = ((f32[4,2,512]{2,1,0:T(2,128)S(1)}, f32[4,2,512]{2,1,0:T(2,128)S(1)}, f32[4,2,512,128]{3,2,1,0:T(8,128)})) conditional(s32[]{:T(128)} %convert_element_type.168, (f32[4,2,512]{2,1,0:T(2,128)S(1)}, f32[4,2,512]{2,1,0:T(2,128)S(1)}, f32[4,2,512,128]{3,2,1,0:T(8,128)}) %tuple.88, (s32[]{:T(128)}, s32[]{:T(128)}, ...), branch_computations={%region_4.4_spmd, %region_5.7_spmd} | conditional | flops 833889280 | bytes 49032288 | solution.py:131
  224.4 2.5 fusion.2
  229.1 4.6 %multiply_add_fusion = f32[4,2,512,128]{3,2,1,0:T(8,128)S(1)} fusion(f32[4,2,512,128]{3,2,1,0:T(8,128)S(1)} %copy-done.2, f32[4,2,512,512]{3,2,1,0:T(8,128)S(1)} %get-tuple-element.211, f32[4,2,512]{2,1,0:T(2,128)S(1)} %max.4, pred[512,512]{0,1:T(8,128)(4,1)S(1)} %broadcast_compare_fusion, f32[4,2,512]{2,1,0:T(2,128)S(1)} %bitcast.134, ...), kind=kOutput, calls=%fused_computation.8 | convolution fusion | flops 548405248 | bytes 13402624 | tf_op jit(solution)/shard_map/while/body/eval_jaxpr/cond/branch_1_fun/hmqk,khd->hmqd/dot_general | solution.py:120
  236.3 10.8 %conditional.3 = ((f32[4,2,512]{2,1,0:T(2,128)S(1)}, f32[4,2,512]{2,1,0:T(2,128)S(1)}, f32[4,2,512,128]{3,2,1,0:T(8,128)})) conditional(s32[]{:T(128)} %convert_element_type.168, (f32[4,2,512]{2,1,0:T(2,128)S(1)}, f32[4,2,512]{2,1,0:T(2,128)S(1)}, f32[4,2,512,128]{3,2,1,0:T(8,128)}) %tuple.88, (s32[]{:T(128)}, s32[]{:T(128)}, ...), branch_computations={%region_4.4_spmd, %region_5.7_spmd} | conditional | flops 833889280 | bytes 49032288 | solution.py:131
  241.2 4.6 %multiply_add_fusion = f32[4,2,512,128]{3,2,1,0:T(8,128)S(1)} fusion(f32[4,2,512,128]{3,2,1,0:T(8,128)S(1)} %copy-done.2, f32[4,2,512,512]{3,2,1,0:T(8,128)S(1)} %get-tuple-element.211, f32[4,2,512]{2,1,0:T(2,128)S(1)} %max.4, pred[512,512]{0,1:T(8,128)(4,1)S(1)} %broadcast_compare_fusion, f32[4,2,512]{2,1,0:T(2,128)S(1)} %bitcast.134, ...), kind=kOutput, calls=%fused_computation.8 | convolution fusion | flops 548405248 | bytes 13402624 | tf_op jit(solution)/shard_map/while/body/eval_jaxpr/cond/branch_1_fun/hmqk,khd->hmqd/dot_general | solution.py:120
  248.4 10.8 %conditional.3 = ((f32[4,2,512]{2,1,0:T(2,128)S(1)}, f32[4,2,512]{2,1,0:T(2,128)S(1)}, f32[4,2,512,128]{3,2,1,0:T(8,128)})) conditional(s32[]{:T(128)} %convert_element_type.168, (f32[4,2,512]{2,1,0:T(2,128)S(1)}, f32[4,2,512]{2,1,0:T(2,128)S(1)}, f32[4,2,512,128]{3,2,1,0:T(8,128)}) %tuple.88, (s32[]{:T(128)}, s32[]{:T(128)}, ...), branch_computations={%region_4.4_spmd, %region_5.7_spmd} | conditional | flops 833889280 | bytes 49032288 | solution.py:131
  253.3 4.6 %multiply_add_fusion = f32[4,2,512,128]{3,2,1,0:T(8,128)S(1)} fusion(f32[4,2,512,128]{3,2,1,0:T(8,128)S(1)} %copy-done.2, f32[4,2,512,512]{3,2,1,0:T(8,128)S(1)} %get-tuple-element.211, f32[4,2,512]{2,1,0:T(2,128)S(1)} %max.4, pred[512,512]{0,1:T(8,128)(4,1)S(1)} %broadcast_compare_fusion, f32[4,2,512]{2,1,0:T(2,128)S(1)} %bitcast.134, ...), kind=kOutput, calls=%fused_computation.8 | convolution fusion | flops 548405248 | bytes 13402624 | tf_op jit(solution)/shard_map/while/body/eval_jaxpr/cond/branch_1_fun/hmqk,khd->hmqd/dot_general | solution.py:120
  260.5 10.8 %conditional.3 = ((f32[4,2,512]{2,1,0:T(2,128)S(1)}, f32[4,2,512]{2,1,0:T(2,128)S(1)}, f32[4,2,512,128]{3,2,1,0:T(8,128)})) conditional(s32[]{:T(128)} %convert_element_type.168, (f32[4,2,512]{2,1,0:T(2,128)S(1)}, f32[4,2,512]{2,1,0:T(2,128)S(1)}, f32[4,2,512,128]{3,2,1,0:T(8,128)}) %tuple.88, (s32[]{:T(128)}, s32[]{:T(128)}, ...), branch_computations={%region_4.4_spmd, %region_5.7_spmd} | conditional | flops 833889280 | bytes 49032288 | solution.py:131
  265.4 4.6 %multiply_add_fusion = f32[4,2,512,128]{3,2,1,0:T(8,128)S(1)} fusion(f32[4,2,512,128]{3,2,1,0:T(8,128)S(1)} %copy-done.2, f32[4,2,512,512]{3,2,1,0:T(8,128)S(1)} %get-tuple-element.211, f32[4,2,512]{2,1,0:T(2,128)S(1)} %max.4, pred[512,512]{0,1:T(8,128)(4,1)S(1)} %broadcast_compare_fusion, f32[4,2,512]{2,1,0:T(2,128)S(1)} %bitcast.134, ...), kind=kOutput, calls=%fused_computation.8 | convolution fusion | flops 548405248 | bytes 13402624 | tf_op jit(solution)/shard_map/while/body/eval_jaxpr/cond/branch_1_fun/hmqk,khd->hmqd/dot_general | solution.py:120
  272.6 10.8 %conditional.3 = ((f32[4,2,512]{2,1,0:T(2,128)S(1)}, f32[4,2,512]{2,1,0:T(2,128)S(1)}, f32[4,2,512,128]{3,2,1,0:T(8,128)})) conditional(s32[]{:T(128)} %convert_element_type.168, (f32[4,2,512]{2,1,0:T(2,128)S(1)}, f32[4,2,512]{2,1,0:T(2,128)S(1)}, f32[4,2,512,128]{3,2,1,0:T(8,128)}) %tuple.88, (s32[]{:T(128)}, s32[]{:T(128)}, ...), branch_computations={%region_4.4_spmd, %region_5.7_spmd} | conditional | flops 833889280 | bytes 49032288 | solution.py:131
  277.5 4.6 %multiply_add_fusion = f32[4,2,512,128]{3,2,1,0:T(8,128)S(1)} fusion(f32[4,2,512,128]{3,2,1,0:T(8,128)S(1)} %copy-done.2, f32[4,2,512,512]{3,2,1,0:T(8,128)S(1)} %get-tuple-element.211, f32[4,2,512]{2,1,0:T(2,128)S(1)} %max.4, pred[512,512]{0,1:T(8,128)(4,1)S(1)} %broadcast_compare_fusion, f32[4,2,512]{2,1,0:T(2,128)S(1)} %bitcast.134, ...), kind=kOutput, calls=%fused_computation.8 | convolution fusion | flops 548405248 | bytes 13402624 | tf_op jit(solution)/shard_map/while/body/eval_jaxpr/cond/branch_1_fun/hmqk,khd->hmqd/dot_general | solution.py:120
  284.7 10.8 %conditional.3 = ((f32[4,2,512]{2,1,0:T(2,128)S(1)}, f32[4,2,512]{2,1,0:T(2,128)S(1)}, f32[4,2,512,128]{3,2,1,0:T(8,128)})) conditional(s32[]{:T(128)} %convert_element_type.168, (f32[4,2,512]{2,1,0:T(2,128)S(1)}, f32[4,2,512]{2,1,0:T(2,128)S(1)}, f32[4,2,512,128]{3,2,1,0:T(8,128)}) %tuple.88, (s32[]{:T(128)}, s32[]{:T(128)}, ...), branch_computations={%region_4.4_spmd, %region_5.7_spmd} | conditional | flops 833889280 | bytes 49032288 | solution.py:131
  289.6 4.6 %multiply_add_fusion = f32[4,2,512,128]{3,2,1,0:T(8,128)S(1)} fusion(f32[4,2,512,128]{3,2,1,0:T(8,128)S(1)} %copy-done.2, f32[4,2,512,512]{3,2,1,0:T(8,128)S(1)} %get-tuple-element.211, f32[4,2,512]{2,1,0:T(2,128)S(1)} %max.4, pred[512,512]{0,1:T(8,128)(4,1)S(1)} %broadcast_compare_fusion, f32[4,2,512]{2,1,0:T(2,128)S(1)} %bitcast.134, ...), kind=kOutput, calls=%fused_computation.8 | convolution fusion | flops 548405248 | bytes 13402624 | tf_op jit(solution)/shard_map/while/body/eval_jaxpr/cond/branch_1_fun/hmqk,khd->hmqd/dot_general | solution.py:120
  296.8 10.8 %conditional.3 = ((f32[4,2,512]{2,1,0:T(2,128)S(1)}, f32[4,2,512]{2,1,0:T(2,128)S(1)}, f32[4,2,512,128]{3,2,1,0:T(8,128)})) conditional(s32[]{:T(128)} %convert_element_type.168, (f32[4,2,512]{2,1,0:T(2,128)S(1)}, f32[4,2,512]{2,1,0:T(2,128)S(1)}, f32[4,2,512,128]{3,2,1,0:T(8,128)}) %tuple.88, (s32[]{:T(128)}, s32[]{:T(128)}, ...), branch_computations={%region_4.4_spmd, %region_5.7_spmd} | conditional | flops 833889280 | bytes 49032288 | solution.py:131
  301.7 4.6 %multiply_add_fusion = f32[4,2,512,128]{3,2,1,0:T(8,128)S(1)} fusion(f32[4,2,512,128]{3,2,1,0:T(8,128)S(1)} %copy-done.2, f32[4,2,512,512]{3,2,1,0:T(8,128)S(1)} %get-tuple-element.211, f32[4,2,512]{2,1,0:T(2,128)S(1)} %max.4, pred[512,512]{0,1:T(8,128)(4,1)S(1)} %broadcast_compare_fusion, f32[4,2,512]{2,1,0:T(2,128)S(1)} %bitcast.134, ...), kind=kOutput, calls=%fused_computation.8 | convolution fusion | flops 548405248 | bytes 13402624 | tf_op jit(solution)/shard_map/while/body/eval_jaxpr/cond/branch_1_fun/hmqk,khd->hmqd/dot_general | solution.py:120
  308.9 10.8 %conditional.3 = ((f32[4,2,512]{2,1,0:T(2,128)S(1)}, f32[4,2,512]{2,1,0:T(2,128)S(1)}, f32[4,2,512,128]{3,2,1,0:T(8,128)})) conditional(s32[]{:T(128)} %convert_element_type.168, (f32[4,2,512]{2,1,0:T(2,128)S(1)}, f32[4,2,512]{2,1,0:T(2,128)S(1)}, f32[4,2,512,128]{3,2,1,0:T(8,128)}) %tuple.88, (s32[]{:T(128)}, s32[]{:T(128)}, ...), branch_computations={%region_4.4_spmd, %region_5.7_spmd} | conditional | flops 833889280 | bytes 49032288 | solution.py:131
  313.8 4.6 %multiply_add_fusion = f32[4,2,512,128]{3,2,1,0:T(8,128)S(1)} fusion(f32[4,2,512,128]{3,2,1,0:T(8,128)S(1)} %copy-done.2, f32[4,2,512,512]{3,2,1,0:T(8,128)S(1)} %get-tuple-element.211, f32[4,2,512]{2,1,0:T(2,128)S(1)} %max.4, pred[512,512]{0,1:T(8,128)(4,1)S(1)} %broadcast_compare_fusion, f32[4,2,512]{2,1,0:T(2,128)S(1)} %bitcast.134, ...), kind=kOutput, calls=%fused_computation.8 | convolution fusion | flops 548405248 | bytes 13402624 | tf_op jit(solution)/shard_map/while/body/eval_jaxpr/cond/branch_1_fun/hmqk,khd->hmqd/dot_general | solution.py:120
  321.0 10.8 %conditional.3 = ((f32[4,2,512]{2,1,0:T(2,128)S(1)}, f32[4,2,512]{2,1,0:T(2,128)S(1)}, f32[4,2,512,128]{3,2,1,0:T(8,128)})) conditional(s32[]{:T(128)} %convert_element_type.168, (f32[4,2,512]{2,1,0:T(2,128)S(1)}, f32[4,2,512]{2,1,0:T(2,128)S(1)}, f32[4,2,512,128]{3,2,1,0:T(8,128)}) %tuple.88, (s32[]{:T(128)}, s32[]{:T(128)}, ...), branch_computations={%region_4.4_spmd, %region_5.7_spmd} | conditional | flops 833889280 | bytes 49032288 | solution.py:131
  325.9 4.6 %multiply_add_fusion = f32[4,2,512,128]{3,2,1,0:T(8,128)S(1)} fusion(f32[4,2,512,128]{3,2,1,0:T(8,128)S(1)} %copy-done.2, f32[4,2,512,512]{3,2,1,0:T(8,128)S(1)} %get-tuple-element.211, f32[4,2,512]{2,1,0:T(2,128)S(1)} %max.4, pred[512,512]{0,1:T(8,128)(4,1)S(1)} %broadcast_compare_fusion, f32[4,2,512]{2,1,0:T(2,128)S(1)} %bitcast.134, ...), kind=kOutput, calls=%fused_computation.8 | convolution fusion | flops 548405248 | bytes 13402624 | tf_op jit(solution)/shard_map/while/body/eval_jaxpr/cond/branch_1_fun/hmqk,khd->hmqd/dot_general | solution.py:120
  333.1 10.8 %conditional.3 = ((f32[4,2,512]{2,1,0:T(2,128)S(1)}, f32[4,2,512]{2,1,0:T(2,128)S(1)}, f32[4,2,512,128]{3,2,1,0:T(8,128)})) conditional(s32[]{:T(128)} %convert_element_type.168, (f32[4,2,512]{2,1,0:T(2,128)S(1)}, f32[4,2,512]{2,1,0:T(2,128)S(1)}, f32[4,2,512,128]{3,2,1,0:T(8,128)}) %tuple.88, (s32[]{:T(128)}, s32[]{:T(128)}, ...), branch_computations={%region_4.4_spmd, %region_5.7_spmd} | conditional | flops 833889280 | bytes 49032288 | solution.py:131
  338.0 4.6 %multiply_add_fusion = f32[4,2,512,128]{3,2,1,0:T(8,128)S(1)} fusion(f32[4,2,512,128]{3,2,1,0:T(8,128)S(1)} %copy-done.2, f32[4,2,512,512]{3,2,1,0:T(8,128)S(1)} %get-tuple-element.211, f32[4,2,512]{2,1,0:T(2,128)S(1)} %max.4, pred[512,512]{0,1:T(8,128)(4,1)S(1)} %broadcast_compare_fusion, f32[4,2,512]{2,1,0:T(2,128)S(1)} %bitcast.134, ...), kind=kOutput, calls=%fused_computation.8 | convolution fusion | flops 548405248 | bytes 13402624 | tf_op jit(solution)/shard_map/while/body/eval_jaxpr/cond/branch_1_fun/hmqk,khd->hmqd/dot_general | solution.py:120
  345.2 10.8 %conditional.3 = ((f32[4,2,512]{2,1,0:T(2,128)S(1)}, f32[4,2,512]{2,1,0:T(2,128)S(1)}, f32[4,2,512,128]{3,2,1,0:T(8,128)})) conditional(s32[]{:T(128)} %convert_element_type.168, (f32[4,2,512]{2,1,0:T(2,128)S(1)}, f32[4,2,512]{2,1,0:T(2,128)S(1)}, f32[4,2,512,128]{3,2,1,0:T(8,128)}) %tuple.88, (s32[]{:T(128)}, s32[]{:T(128)}, ...), branch_computations={%region_4.4_spmd, %region_5.7_spmd} | conditional | flops 833889280 | bytes 49032288 | solution.py:131
  350.1 4.6 %multiply_add_fusion = f32[4,2,512,128]{3,2,1,0:T(8,128)S(1)} fusion(f32[4,2,512,128]{3,2,1,0:T(8,128)S(1)} %copy-done.2, f32[4,2,512,512]{3,2,1,0:T(8,128)S(1)} %get-tuple-element.211, f32[4,2,512]{2,1,0:T(2,128)S(1)} %max.4, pred[512,512]{0,1:T(8,128)(4,1)S(1)} %broadcast_compare_fusion, f32[4,2,512]{2,1,0:T(2,128)S(1)} %bitcast.134, ...), kind=kOutput, calls=%fused_computation.8 | convolution fusion | flops 548405248 | bytes 13402624 | tf_op jit(solution)/shard_map/while/body/eval_jaxpr/cond/branch_1_fun/hmqk,khd->hmqd/dot_general | solution.py:120
  357.3 10.8 %conditional.3 = ((f32[4,2,512]{2,1,0:T(2,128)S(1)}, f32[4,2,512]{2,1,0:T(2,128)S(1)}, f32[4,2,512,128]{3,2,1,0:T(8,128)})) conditional(s32[]{:T(128)} %convert_element_type.168, (f32[4,2,512]{2,1,0:T(2,128)S(1)}, f32[4,2,512]{2,1,0:T(2,128)S(1)}, f32[4,2,512,128]{3,2,1,0:T(8,128)}) %tuple.88, (s32[]{:T(128)}, s32[]{:T(128)}, ...), branch_computations={%region_4.4_spmd, %region_5.7_spmd} | conditional | flops 833889280 | bytes 49032288 | solution.py:131
  362.2 4.6 %multiply_add_fusion = f32[4,2,512,128]{3,2,1,0:T(8,128)S(1)} fusion(f32[4,2,512,128]{3,2,1,0:T(8,128)S(1)} %copy-done.2, f32[4,2,512,512]{3,2,1,0:T(8,128)S(1)} %get-tuple-element.211, f32[4,2,512]{2,1,0:T(2,128)S(1)} %max.4, pred[512,512]{0,1:T(8,128)(4,1)S(1)} %broadcast_compare_fusion, f32[4,2,512]{2,1,0:T(2,128)S(1)} %bitcast.134, ...), kind=kOutput, calls=%fused_computation.8 | convolution fusion | flops 548405248 | bytes 13402624 | tf_op jit(solution)/shard_map/while/body/eval_jaxpr/cond/branch_1_fun/hmqk,khd->hmqd/dot_general | solution.py:120
  369.4 10.8 %conditional.3 = ((f32[4,2,512]{2,1,0:T(2,128)S(1)}, f32[4,2,512]{2,1,0:T(2,128)S(1)}, f32[4,2,512,128]{3,2,1,0:T(8,128)})) conditional(s32[]{:T(128)} %convert_element_type.168, (f32[4,2,512]{2,1,0:T(2,128)S(1)}, f32[4,2,512]{2,1,0:T(2,128)S(1)}, f32[4,2,512,128]{3,2,1,0:T(8,128)}) %tuple.88, (s32[]{:T(128)}, s32[]{:T(128)}, ...), branch_computations={%region_4.4_spmd, %region_5.7_spmd} | conditional | flops 833889280 | bytes 49032288 | solution.py:131
  374.3 4.6 %multiply_add_fusion = f32[4,2,512,128]{3,2,1,0:T(8,128)S(1)} fusion(f32[4,2,512,128]{3,2,1,0:T(8,128)S(1)} %copy-done.2, f32[4,2,512,512]{3,2,1,0:T(8,128)S(1)} %get-tuple-element.211, f32[4,2,512]{2,1,0:T(2,128)S(1)} %max.4, pred[512,512]{0,1:T(8,128)(4,1)S(1)} %broadcast_compare_fusion, f32[4,2,512]{2,1,0:T(2,128)S(1)} %bitcast.134, ...), kind=kOutput, calls=%fused_computation.8 | convolution fusion | flops 548405248 | bytes 13402624 | tf_op jit(solution)/shard_map/while/body/eval_jaxpr/cond/branch_1_fun/hmqk,khd->hmqd/dot_general | solution.py:120
  381.5 10.8 %conditional.3 = ((f32[4,2,512]{2,1,0:T(2,128)S(1)}, f32[4,2,512]{2,1,0:T(2,128)S(1)}, f32[4,2,512,128]{3,2,1,0:T(8,128)})) conditional(s32[]{:T(128)} %convert_element_type.168, (f32[4,2,512]{2,1,0:T(2,128)S(1)}, f32[4,2,512]{2,1,0:T(2,128)S(1)}, f32[4,2,512,128]{3,2,1,0:T(8,128)}) %tuple.88, (s32[]{:T(128)}, s32[]{:T(128)}, ...), branch_computations={%region_4.4_spmd, %region_5.7_spmd} | conditional | flops 833889280 | bytes 49032288 | solution.py:131
  386.4 4.6 %multiply_add_fusion = f32[4,2,512,128]{3,2,1,0:T(8,128)S(1)} fusion(f32[4,2,512,128]{3,2,1,0:T(8,128)S(1)} %copy-done.2, f32[4,2,512,512]{3,2,1,0:T(8,128)S(1)} %get-tuple-element.211, f32[4,2,512]{2,1,0:T(2,128)S(1)} %max.4, pred[512,512]{0,1:T(8,128)(4,1)S(1)} %broadcast_compare_fusion, f32[4,2,512]{2,1,0:T(2,128)S(1)} %bitcast.134, ...), kind=kOutput, calls=%fused_computation.8 | convolution fusion | flops 548405248 | bytes 13402624 | tf_op jit(solution)/shard_map/while/body/eval_jaxpr/cond/branch_1_fun/hmqk,khd->hmqd/dot_general | solution.py:120
  393.6 10.8 %conditional.3 = ((f32[4,2,512]{2,1,0:T(2,128)S(1)}, f32[4,2,512]{2,1,0:T(2,128)S(1)}, f32[4,2,512,128]{3,2,1,0:T(8,128)})) conditional(s32[]{:T(128)} %convert_element_type.168, (f32[4,2,512]{2,1,0:T(2,128)S(1)}, f32[4,2,512]{2,1,0:T(2,128)S(1)}, f32[4,2,512,128]{3,2,1,0:T(8,128)}) %tuple.88, (s32[]{:T(128)}, s32[]{:T(128)}, ...), branch_computations={%region_4.4_spmd, %region_5.7_spmd} | conditional | flops 833889280 | bytes 49032288 | solution.py:131
  398.5 4.6 %multiply_add_fusion = f32[4,2,512,128]{3,2,1,0:T(8,128)S(1)} fusion(f32[4,2,512,128]{3,2,1,0:T(8,128)S(1)} %copy-done.2, f32[4,2,512,512]{3,2,1,0:T(8,128)S(1)} %get-tuple-element.211, f32[4,2,512]{2,1,0:T(2,128)S(1)} %max.4, pred[512,512]{0,1:T(8,128)(4,1)S(1)} %broadcast_compare_fusion, f32[4,2,512]{2,1,0:T(2,128)S(1)} %bitcast.134, ...), kind=kOutput, calls=%fused_computation.8 | convolution fusion | flops 548405248 | bytes 13402624 | tf_op jit(solution)/shard_map/while/body/eval_jaxpr/cond/branch_1_fun/hmqk,khd->hmqd/dot_general | solution.py:120
  408.9 3.6 all-to-all-start
  413.1 7.6 %all-to-all-done = bf16[2,256,1024]{2,1,0:T(8,128)(2,1)S(1)} async-done(((bf16[2,256,1024]{2,1,0:T(8,128)(2,1)}), bf16[2,256,1024]{2,1,0:T(8,128)(2,1)S(1)}, u32[]{:S(2)}, u32[]{:S(2)}) %all-to-all-start) | async-done | bytes 1048608 | tf_op jit(solution)/shard_map/all_to_all | solution.py:171
  421.2 6.8 %fusion.23 = bf16[256,2048]{1,0:T(8,128)(2,1)} fusion(bf16[2,2,512,2048]{3,2,1,0:T(8,128)(2,1)} %bitcast.122, bf16[256,2,2,512]{0,3,2,1:T(8,128)(2,1)S(1)} %bitcast.126), kind=kOutput, calls=%fused_computation.31 | convolution fusion | flops 2148007936 | bytes 10485760 | tf_op jit(solution)/shard_map/rtcj,ctjd->rd/dot_general | solution.py:173
  (276 shorter events, 123.6 us)
Async XLA Ops:
  7.2 43.0 %copy-start = (bf16[2048,512]{1,0:T(8,128)(2,1)S(1)}, bf16[2048,512]{1,0:T(8,128)(2,1)}, u32[]{:S(2)}) copy-start(bf16[2048,512]{1,0:T(8,128)(2,1)} %param.20) | copy-start | bytes 6291460
  7.2 38.5 %copy-start.15 = (f32[2048]{0:T(1024)S(1)}, f32[2048]{0:T(1024)}, u32[]{:S(2)}) copy-start(f32[2048]{0:T(1024)} %param.19) | copy-start | bytes 24580
  7.2 36.2 %all-gather.4.cloned.1.call-start = ((), (), s32[]{:S(2)}) async-start(), calls=%async_computation.1 | async-start | bytes 3145728 | tf_op jit(solution)/shard_map/all_gather | solution.py:72
  7.9 114.9 %all-gather.8.cloned.1.call-start = ((), (), s32[]{:S(2)}) async-start(), calls=%async_computation.3 | async-start | bytes 8912896 | tf_op jit(solution)/shard_map/all_gather | solution.py:96
  43.4 2.2 copy-start.4
  49.7 151.6 %all-gather.6.cloned.1.call-start = ((), (), s32[]{:S(2)}) async-start(), calls=%async_computation.2 | async-start | bytes 8912896 | tf_op jit(solution)/shard_map/all_gather | solution.py:95
  50.1 3.2 copy-start.5
  50.2 3.2 copy-start.13
  53.3 1.5 copy-start.10
  56.5 4.0 copy-start.6
  56.5 4.0 copy-start.14
  62.0 3.4 collective-permute-start
  65.6 9.4 %copy-start.8 = (f32[512]{0:T(512)S(1)}, f32[512]{0:T(512)}, u32[]{:S(2)}) copy-start(f32[512]{0:T(512)} %param.30) | copy-start | bytes 6148
  65.7 9.4 %copy-start.9 = (f32[512]{0:T(512)S(1)}, f32[512]{0:T(512)}, u32[]{:S(2)}) copy-start(f32[512]{0:T(512)} %param.29) | copy-start | bytes 6148
  210.8 193.7 %copy-start.12 = (f32[4]{0:T(128)S(1)}, f32[4]{0:T(128)}, u32[]{:S(2)}) copy-start(f32[4]{0:T(128)} %param.26) | copy-start | bytes 52
  214.9 2.1 copy-start.2
  221.6 1.3 copy-start.3
  227.0 2.1 copy-start.2
  233.7 1.3 copy-start.3
  239.1 2.1 copy-start.2
  251.2 2.1 copy-start.2
  257.9 1.3 copy-start.3
  263.3 2.1 copy-start.2
  270.0 1.3 copy-start.3
  275.4 2.1 copy-start.2
  282.1 1.3 copy-start.3
  287.5 2.1 copy-start.2
  294.2 1.3 copy-start.3
  299.6 2.1 copy-start.2
  306.3 1.3 copy-start.3
  311.7 2.1 copy-start.2
  318.4 1.3 copy-start.3
  323.8 2.1 copy-start.2
  330.5 1.3 copy-start.3
  335.9 2.1 copy-start.2
  342.6 1.3 copy-start.3
  348.0 2.1 copy-start.2
  354.7 1.3 copy-start.3
  360.1 2.1 copy-start.2
  366.8 1.3 copy-start.3
  372.2 2.1 copy-start.2
  378.9 1.3 copy-start.3
  384.3 2.1 copy-start.2
  391.0 1.3 copy-start.3
  396.4 2.1 copy-start.2
  404.4 2.3 copy-start.11
  408.9 11.8 %all-to-all-start = ((bf16[2,256,1024]{2,1,0:T(8,128)(2,1)}), bf16[2,256,1024]{2,1,0:T(8,128)(2,1)S(1)}, u32[]{:S(2)}, u32[]{:S(2)}) async-start(bf16[2,256,1024]{2,1,0:T(8,128)(2,1)} %pad_maximum_fusion), calls=%async_computation | async-start | bytes 2097152 | tf_op jit(solution)/shard_map/all_to_all | solution.py:171
  421.2 6.9 %copy-start.1 = (bf16[2048,512]{1,0:T(8,128)(2,1)S(1)}, bf16[2048,512]{1,0:T(8,128)(2,1)}, u32[]{:S(2)}) copy-start(bf16[2048,512]{1,0:T(8,128)(2,1)} %param.20) | copy-start | bytes 6291460
  (3 other events, 3.9 us)
Sparse Core Ops, SparseCore 0:
  9.5 33.8 all-gather.3
  49.9 72.8 all-gather.7
  125.5 75.8 all-gather.5
where the time goes:
time: 437 us; the launch traced here: 435 us
  waiting for transfers between devices  164 us (38%)
  matrix products  134 us (31%)
  other arithmetic  50.9 us (12%)
  local copies, waits for them, and re-layouts  50.6 us (12%)
  between operations  14.1 us (3%)
  loops' own time  11.9 us (3%)
  starting transfers between devices  4.99 us (1%)
    dot_general x16, matrix products, compute(): jnp.einsum('hmqk,khd->hmqd', probs.astype(jnp.bfloat16), value_block, pre...  73.1 us
    all_gather x1, waiting for transfers between devices, per_device(): key_piece = lax.all_gather(rk, 'sp', axis=0, tiled=True)  71 us
    all_gather x1, waiting for transfers between devices, per_device(): value_piece = lax.all_gather(values, 'sp', axis=0, tiled=True)  47.3 us
    dot_general x16, matrix products, compute(): jnp.einsum('hmqd,khmd->hmqk', rq, key_block, preferred_element_type=jnp.f...  40.7 us
    all_gather x1, waiting for transfers between devices, per_device(): projected = project(lax.all_gather(tokens, 'tp', axis=0, tiled=True))  35.5 us
    reduce_sum x16, other arithmetic, compute(): totals = totals * factor + jnp.sum(probs, axis=-1)  32.8 us
    cond x80, local copies, waits for them, and re-layouts  21.3 us
    dot_general x5, matrix products, project(): jnp.dot(normed, matrix, preferred_element_type=jnp.float32)  13.1 us
  transfers between devices with their start and end apart: 5, of which 5 were waited for; matrix products, arithmetic and copies ran while one was open for 6% of the time, Pallas kernels for 0%

commit v1 on v0

v1 whole, which is shorter than its diff:
```python
import math

import jax
import jax.numpy as jnp
from jax import lax
from jax.experimental import pallas as pl
from jax.experimental.pallas import tpu as pltpu
from jax.sharding import PartitionSpec as P

MESH = pl.DeviceIdType.MESH
NEG = -1e30


def from_behind(value, axis, steps):
    count = lax.axis_size(axis)
    leading, last = (max(0, -steps), min(count, count - steps))
    return lax.ppermute(value, axis, [(source, source + steps) for source in range(leading, last)])


def spread_kernel(ways, group, q_ref, kv_ref, qo_ref, kvo_ref, qsend, qrecv, ksend, kfwd, krelay, krecv, local):
    me = lax.axis_index("sp")
    a = me // group
    g = me % group
    cores = 2 if group % 2 == 0 else 1
    half = group // cores
    mate = a * group + (g + 1 - 2 * (g % 2)) if cores == 2 else me

    def same(d):
        return (g + d * cores) % group

    peers = [lax.rem(a + d, ways) * group + g for d in range(1, ways)]
    peers += [a * group + same(d) for d in range(1, half)]
    if cores == 2:
        peers.append(mate)
    barrier = pltpu.get_barrier_semaphore()
    for peer in peers:
        pl.semaphore_signal(barrier, inc=1, device_id={"sp": peer}, device_id_type=MESH)
    pl.semaphore_wait(barrier, len(peers))

    def kv_copy(src, slot, send, peer):
        return pltpu.make_async_remote_copy(
            src_ref=src, dst_ref=kvo_ref.at[slot], send_sem=send, recv_sem=krecv.at[slot],
            device_id={"sp": peer}, device_id_type=MESH)

    sends = []
    locals_ = [
        pltpu.make_async_copy(kv_ref.at[a], kvo_ref.at[me], local.at[0]),
        pltpu.make_async_copy(q_ref.at[a], qo_ref.at[a], local.at[1]),
    ]
    for c in locals_:
        c.start()
    order = list(range(1, ways))
    for d in order:
        h = lax.rem(a + d, ways)
        c = kv_copy(kv_ref.at[h], me, ksend.at[d - 1], h * group + g)
        c.start()
        sends.append(c)

    def forward(d):
        src_a = lax.rem(a + ways - d, ways)
        slot = src_a * group + g
        if d:
            kv_copy(kvo_ref.at[slot], slot, ksend.at[d - 1], me).wait_recv()
            src = kvo_ref.at[slot]
        else:
            src = kv_ref.at[a]
        n = 0
        for e in range(1, half):
            c = kv_copy(src, slot, kfwd.at[d, n], a * group + same(e))
            c.start()
            sends.append(c)
            n += 1
        if cores == 2:
            c = kv_copy(src, slot, kfwd.at[d, n], mate)
            c.start()
            sends.append(c)

    def relay(d):
        src_a = lax.rem(a + ways - d, ways)
        for e in range(1, half):
            slot = src_a * group + same(e)
            kv_copy(kvo_ref.at[slot], slot, krelay.at[d, e - 1], mate).wait_recv()
            if cores == 2:
                c = kv_copy(kvo_ref.at[slot], slot, krelay.at[d, e - 1], mate)
                c.start()
                sends.append(c)

    forward(0)
    for d in order:
        h = lax.rem(a + d, ways)
        c = pltpu.make_async_remote_copy(
            src_ref=q_ref.at[h], dst_ref=qo_ref.at[a], send_sem=qsend.at[d - 1], recv_sem=qrecv.at[a],
            device_id={"sp": h * group + g}, device_id_type=MESH)
        c.start()
        sends.append(c)
    for d in range(1, ways):
        forward(d)
        relay(d - 1)
    relay(ways - 1)
    if cores == 2:
        for d in range(ways):
            src_a = lax.rem(a + ways - d, ways)
            for e in range(half):
                slot = src_a * group + (g + 1 - 2 * (g % 2) + e * cores) % group
                kv_copy(kvo_ref.at[slot], slot, krelay.at[0, 0], mate).wait_recv()
    for d in range(1, ways):
        src_a = lax.rem(a + ways - d, ways)
        pltpu.make_async_remote_copy(
            src_ref=q_ref.at[a], dst_ref=qo_ref.at[src_a], send_sem=qsend.at[d - 1],
            recv_sem=qrecv.at[src_a], device_id={"sp": me}, device_id_type=MESH).wait_recv()
    for c in sends:
        c.wait_send()
    for c in locals_:
        c.wait()


def spread(q, kv, ways, group):
    cores = 2 if group % 2 == 0 else 1
    half = group // cores
    any_ = pl.BlockSpec(memory_space=pl.ANY)
    n = max(ways - 1, 1)
    return pl.pallas_call(
        lambda *refs: spread_kernel(ways, group, *refs),
        out_shape=(
            jax.ShapeDtypeStruct(q.shape, q.dtype),
            jax.ShapeDtypeStruct((ways * group,) + kv.shape[1:], kv.dtype),
        ),
        in_specs=[any_, any_],
        out_specs=(any_, any_),
        scratch_shapes=[
            pltpu.SemaphoreType.DMA((n,)),
            pltpu.SemaphoreType.DMA((ways,)),
            pltpu.SemaphoreType.DMA((n,)),
            pltpu.SemaphoreType.DMA((ways, half)),
            pltpu.SemaphoreType.DMA((ways, max(half - 1, 1))),
            pltpu.SemaphoreType.DMA((ways * group,)),
            pltpu.SemaphoreType.DMA((2,)),
        ],
        compiler_params=pltpu.CompilerParams(collective_id=1, has_side_effects=True),
        name="spread",
    )(q, kv)


def collect_kernel(ways, group, tp, att_ref, lt_ref, conv_ref, ao_ref, lo_ref, co_ref, asend, arecv, lsend, lrecv, csend, crecv, local):
    me = lax.axis_index("sp")
    t = lax.axis_index("tp")
    a = me // group
    g = me % group
    vdim = att_ref.shape[-1]
    cch = conv_ref.shape[-1]

    def coords(i):
        dt, da = i % tp, i // tp
        return lax.rem(a + da, ways), lax.rem(t + dt, tp)

    total = ways * tp
    barrier = pltpu.get_barrier_semaphore()
    for i in range(1, total):
        pa, pt = coords(i)
        pl.semaphore_signal(barrier, inc=1, device_id={"sp": pa * group + g, "tp": pt}, device_id_type=MESH)
    pl.semaphore_wait(barrier, total - 1)

    head = t * ways + a
    sends = []
    for i in list(range(total - 1, 0, -1)):
        pa, pt = coords(i)
        dev = {"sp": pa * group + g, "tp": pt}
        c = pltpu.make_async_remote_copy(
            src_ref=att_ref.at[pa, pt], dst_ref=ao_ref.at[head],
            send_sem=asend.at[i], recv_sem=arecv.at[head], device_id=dev, device_id_type=MESH)
        c.start()
        sends.append(c)
    for i in range(1, tp):
        pa, pt = coords(i)
        c = pltpu.make_async_remote_copy(
            src_ref=conv_ref.at[pt], dst_ref=co_ref.at[t],
            send_sem=csend.at[i], recv_sem=crecv.at[t],
            device_id={"sp": me, "tp": pt}, device_id_type=MESH)
        c.start()
        sends.append(c)
    for i in range(1, ways):
        pa = lax.rem(a + i, ways)
        c = pltpu.make_async_remote_copy(
            src_ref=lt_ref.at[pa], dst_ref=lo_ref.at[a], send_sem=lsend.at[i], recv_sem=lrecv.at[a],
            device_id={"sp": pa * group + g, "tp": t}, device_id_type=MESH)
        c.start()
        sends.append(c)
    mine = [
        pltpu.make_async_copy(att_ref.at[a, t], ao_ref.at[head], local.at[0]),
        pltpu.make_async_copy(conv_ref.at[t], co_ref.at[t], local.at[1]),
        pltpu.make_async_copy(lt_ref.at[a], lo_ref.at[a], local.at[2]),
    ]
    for c in mine:
        c.start()
    for i in range(1, total):
        pa, pt = coords(i)
        h = pt * ways + pa
        pltpu.make_async_remote_copy(
            src_ref=att_ref.at[a, t], dst_ref=ao_ref.at[h],
            send_sem=asend.at[i], recv_sem=arecv.at[h],
            device_id={"sp": me, "tp": t}, device_id_type=MESH).wait_recv()
    for i in range(1, tp):
        pa, pt = coords(i)
        pltpu.make_async_remote_copy(
            src_ref=conv_ref.at[t], dst_ref=co_ref.at[pt],
            send_sem=csend.at[i], recv_sem=crecv.at[pt],
            device_id={"sp": me, "tp": t}, device_id_type=MESH).wait_recv()
    for i in range(1, ways):
        pa = lax.rem(a + i, ways)
        pltpu.make_async_remote_copy(
            src_ref=lt_ref.at[a], dst_ref=lo_ref.at[pa], send_sem=lsend.at[i], recv_sem=lrecv.at[pa],
            device_id={"sp": me, "tp": t}, device_id_type=MESH).wait_recv()
    for c in sends:
        c.wait_send()
    for c in mine:
        c.wait()


def collect(att, lt, conv, ways, group, tp):
    any_ = pl.BlockSpec(memory_space=pl.ANY)
    rows, vdim = att.shape[2:]
    total = ways * tp
    return pl.pallas_call(
        lambda *refs: collect_kernel(ways, group, tp, *refs),
        out_shape=(
            jax.ShapeDtypeStruct((total, rows, vdim), att.dtype),
            jax.ShapeDtypeStruct(lt.shape, lt.dtype),
            jax.ShapeDtypeStruct(conv.shape, conv.dtype),
        ),
        in_specs=[any_] * 3,
        out_specs=(any_,) * 3,
        scratch_shapes=[
            pltpu.SemaphoreType.DMA((total,)),
            pltpu.SemaphoreType.DMA((total,)),
            pltpu.SemaphoreType.DMA((ways,)),
            pltpu.SemaphoreType.DMA((ways,)),
            pltpu.SemaphoreType.DMA((tp,)),
            pltpu.SemaphoreType.DMA((tp,)),
            pltpu.SemaphoreType.DMA((3,)),
        ],
        compiler_params=pltpu.CompilerParams(collective_id=2, has_side_effects=True),
        name="collect",
    )(att, lt, conv)


def attention(place, lam, head_gain, qt, kv, tile=512):
    ways, qdim, rows = qt.shape
    hd = qdim // 2
    blocks = kv.shape[0]
    vdim = head_gain.shape[0]
    group = blocks // ways
    tile = min(tile, rows)
    tiles = rows // tile

    def kernel(place_ref, lam_ref, gain_ref, q_ref, kv_ref, o_ref, lt_ref):
        i = pl.program_id(0)
        s = pl.program_id(1)
        chunk = i * group + place_ref[0]
        qs = [q_ref[0, m * hd:(m + 1) * hd, :] for m in range(2)]

        def step(j, carry, masked):
            out = []
            kb = kv_ref[j, :rows]
            vb = jnp.concatenate(
                [kv_ref[j, rows + b * vdim:rows + (b + 1) * vdim] for b in range(rows // 128)], axis=1)
            for m in range(2):
                top, tot, acc = carry[m]
                sc = jnp.dot(kb[:, m * hd:(m + 1) * hd], qs[m], preferred_element_type=jnp.float32)
                if masked:
                    kp = lax.broadcasted_iota(jnp.int32, sc.shape, 0)
                    qp = lax.broadcasted_iota(jnp.int32, sc.shape, 1) + s * tile
                    sc = jnp.where(kp <= qp, sc, NEG)
                new = jnp.maximum(top, jnp.max(sc, axis=0, keepdims=True))
                p = jnp.exp(sc - new)
                f = jnp.exp(top - new)
                tot = tot * f + jnp.sum(p, axis=0, keepdims=True)
                acc = acc * f + jnp.dot(vb, p.astype(jnp.bfloat16), preferred_element_type=jnp.float32)
                out.append((new, tot, acc))
            return tuple(out)

        one = (jnp.full((1, tile), NEG, jnp.float32), jnp.zeros((1, tile), jnp.float32),
               jnp.zeros((vdim, tile), jnp.float32))
        carry = step(chunk, (one, one), True)
        carry = lax.fori_loop(0, chunk, lambda j, c: step(j, c, False), carry)
        (t0, l0, a0), (t1, l1, a1) = carry
        heads = a0 / l0 - lam_ref[0] * a1 / l1
        heads = heads * lax.rsqrt(jnp.mean(heads * heads, axis=0, keepdims=True) + 1e-06) * gain_ref[...]
        o_ref[0] = heads.T.astype(jnp.bfloat16)
        lt_ref[0, 0:1, :] = t0 + jnp.log(l0)
        lt_ref[0, 1:2, :] = t1 + jnp.log(l1)

    smem = pl.BlockSpec(memory_space=pltpu.SMEM)
    return pl.pallas_call(
        kernel,
        grid=(ways, tiles),
        out_shape=(
            jax.ShapeDtypeStruct((ways, rows, vdim), jnp.bfloat16),
            jax.ShapeDtypeStruct((ways, 2, rows), jnp.float32),
        ),
        in_specs=[
            smem, smem,
            pl.BlockSpec((vdim, 1), lambda i, s: (0, 0)),
            pl.BlockSpec((1, qdim, tile), lambda i, s: (i, 0, s)),
            pl.BlockSpec(kv.shape, lambda i, s: (0, 0, 0)),
        ],
        out_specs=(
            pl.BlockSpec((1, tile, vdim), lambda i, s: (i, s, 0)),
            pl.BlockSpec((1, 2, tile), lambda i, s: (i, 0, s)),
        ),
        compiler_params=pltpu.CompilerParams(vmem_limit_bytes=50 << 20),
        name="attend",
    )(place, lam, head_gain.reshape(-1, 1), qt, kv)


def prepare_t(raw, qk_gain, cosine, sine):
    values = raw.astype(jnp.float32)
    values = values * lax.rsqrt(jnp.mean(values * values, axis=2, keepdims=True) + 1e-06)
    values = values * qk_gain[None, :, :, None]
    half = raw.shape[2] // 2
    first, second = values[:, :, :half], values[:, :, half:]
    return jnp.concatenate(
        [first * cosine - second * sine, second * cosine + first * sine], axis=2
    ).astype(jnp.bfloat16)


def per_device(
    tokens, norm_gain, query_weight, key_weight, value_weight, glu_value_weight, glu_gate_weight,
    qk_gain, mix_lambda, head_gain, conv_kernel, channel_gain, channel_shift, output_weight,
):
    head_size = qk_gain.shape[1]
    heads_here = mix_lambda.shape[0]
    value_size = head_gain.shape[0]
    kernel_len = conv_kernel.shape[0]
    conv_here = conv_kernel.shape[1]
    width = tokens.shape[1]
    sp = lax.axis_size("sp")
    tp = lax.axis_size("tp")
    me = lax.axis_index("sp")
    t = lax.axis_index("tp")
    ways = heads_here
    group = sp // ways
    own = tokens.shape[0]
    rows = own * tp

    def norm(piece):
        inputs = piece.astype(jnp.float32)
        return (
            inputs * lax.rsqrt(jnp.mean(inputs * inputs, axis=-1, keepdims=True) + 1e-06) * norm_gain
        ).astype(jnp.bfloat16)

    others = [tokens] + [
        lax.ppermute(tokens, "tp", [(i, (i - d) % tp) for i in range(tp)]) for d in range(1, tp)
    ]
    if tp == 2:
        other = others[1]
        normed = norm(jnp.concatenate([jnp.where(t == 0, tokens, other), jnp.where(t == 0, other, tokens)], axis=0))
    else:
        stacked = jnp.stack(others)
        normed = norm(jnp.concatenate(
            [lax.dynamic_index_in_dim(stacked, (j - t) % tp, 0, keepdims=False) for j in range(tp)], axis=0))

    def turned(matrix):
        return lax.dot_general(matrix, normed, (((0,), (1,)), ((), ())), preferred_element_type=jnp.float32).astype(jnp.bfloat16)

    def plain(matrix):
        return jnp.dot(normed, matrix, preferred_element_type=jnp.float32).astype(jnp.bfloat16)

    positions = (me * rows + jnp.arange(rows, dtype=jnp.int32)).astype(jnp.float32)
    inverse = 10000.0 ** (-jnp.arange(0, head_size // 2, dtype=jnp.float32) * 2.0 / head_size)
    angles = positions[None, :] * inverse[:, None]
    cosine, sine = jnp.cos(angles)[None, None], jnp.sin(angles)[None, None]
    shape = (heads_here, 2, head_size, rows)
    rq = prepare_t(turned(query_weight).reshape(shape), qk_gain, cosine, sine) * jnp.bfloat16(head_size ** -0.5)
    rk = prepare_t(turned(key_weight).reshape(shape), qk_gain, cosine, sine)
    qt = rq.reshape(heads_here, 2 * head_size, rows)
    kk = jnp.transpose(rk.reshape(heads_here, 2 * head_size, rows), (0, 2, 1))
    vt = turned(value_weight).reshape(heads_here, value_size, rows)
    kv = jnp.concatenate([kk, vt.reshape(heads_here, value_size, rows // 128, 128).transpose(0, 2, 1, 3).reshape(heads_here, -1, 128)], axis=1)
    qall, kvall = spread(qt, kv, ways, group)

    glu_a, glu_g = plain(glu_value_weight), plain(glu_gate_weight)
    gated = (glu_a.astype(jnp.float32) * jax.nn.sigmoid(glu_g.astype(jnp.float32))).astype(jnp.bfloat16)
    earlier = from_behind(gated[rows - (kernel_len - 1):], "sp", 1)
    extended = jnp.concatenate([earlier, gated], axis=0).astype(jnp.float32)
    convolved = jnp.zeros((rows, conv_here), jnp.float32)
    for step in range(kernel_len):
        convolved = convolved + conv_kernel[step][None, :] * extended[step:step + rows]
    plain_sum, square_sum = lax.psum(
        (jnp.sum(convolved, axis=1), jnp.sum(convolved * convolved, axis=1)), "tp"
    )
    channels = conv_here * tp
    middle = (plain_sum / channels)[:, None]
    spread_ = (square_sum / channels)[:, None] - middle * middle
    conv_out = jax.nn.silu(
        (convolved - middle) * lax.rsqrt(spread_ + 1e-05) * channel_gain + channel_shift
    ).astype(jnp.bfloat16)

    place = (me % group).astype(jnp.int32).reshape(1)
    lam = lax.dynamic_slice(mix_lambda, (me // group,), (1,))
    att, lt = attention(place, lam, head_gain, qall, kvall)
    ao, lo, co = collect(
        att.reshape(ways, tp, own, value_size), lt, conv_out.reshape(tp, own, conv_here), ways, group, tp)
    heads = ways * tp
    merged = jnp.concatenate([
        jnp.transpose(ao, (1, 0, 2)).reshape(own, heads * value_size),
        jnp.transpose(co, (1, 0, 2)).reshape(own, channels)], axis=1)
    mixed = jnp.dot(merged, output_weight, preferred_element_type=jnp.float32).astype(jnp.bfloat16)
    return (mixed, jnp.transpose(lo, (1, 0, 2)))


def solution(mesh):
    placed = (
        P(("sp", "tp"), None), P(), P(None, "tp"), P(None, "tp"), P(None, "tp"), P(None, "tp"), P(None, "tp"),
        P(), P("tp"), P(), P(None, "tp"), P("tp"), P("tp"), P(),
    )
    return jax.shard_map(
        per_device,
        mesh=mesh,
        in_specs=placed,
        out_specs=(P(("sp", "tp"), None), P(None, "tp", "sp")),
        check_vma=False,
    )
```

time: 437 us -> 191 us (0.44)
  waiting for transfers between devices: 164 us -> 17.4 us
  matrix products: 134 us -> 16.4 us
  Pallas kernels: 0 us -> 115 us
  other arithmetic: 50.9 us -> 14.4 us
  local copies, waits for them, and re-layouts: 50.6 us -> 16.5 us
  between operations: 14.1 us -> 1.36 us
  loops' own time: 11.9 us -> 0 us
    all_gather x3 -> x0, waiting for transfers between devices: 154 us -> none  [the longest x1 71 us: per_device(): key_piece = lax.all_gather(rk, 'sp', axis=0, tiled=True)]
    dot_general x38 -> x6, matrix products: 134 us -> 16.4 us  [the longest x3 6.94 us: turned(): lax.dot_general(matrix, normed, (((0,), (1,)), ((), ())), preferred_eleme...]
    pallas_call x0 -> x3, Pallas kernels: none -> 115 us  [the longest x1 52.5 us: attention(): pl.pallas_call(kernel, grid=(ways, tiles), out_shape=(jax.ShapeDtypeStruc...]
    reduce_sum x18 -> x1, other arithmetic: 37.3 us -> 0.48 us  [norm(): jnp.mean(inputs * inputs, axis=-1, keepdims=True) + 1e-06]
    cond x80 -> x0, local copies, waits for them, and re-layouts: 21.3 us -> none
    ppermute x0 -> x1, waiting for transfers between devices: none -> 17.4 us  [per_device(): lax.ppermute(tokens, 'tp', [(i, (i - d) % tp) for i in range(tp)])]
    another operation x17 -> x0, loops' own time: 11.9 us -> none  [the longest x1 10.4 us: per_device(): lax.scan(advance, carry, (key_blocks, value_blocks, jnp.arange(blocks, dt...]
    dynamic_slice x16 -> x1, local copies, waits for them, and re-layouts: 9.85 us -> 1.27 us  [per_device(): lam = lax.dynamic_slice(mix_lambda, (me // group,), (1,))]
  transfers between devices with their start and end apart: 5 -> 2, of which waited for: 5 -> 1; matrix products, arithmetic and copies ran while one was open for 6% -> 12% of each run, Pallas kernels for 0% -> 54%
where the time goes in v1:
time: 191 us; the launch traced here: 188 us
  Pallas kernels  115 us (60%)
  waiting for transfers between devices  17.4 us (9%)
  local copies, waits for them, and re-layouts  16.5 us (9%)
  matrix products  16.4 us (9%)
  other arithmetic  14.4 us (8%)
  blocking collectives  4 us (2%)
  starting transfers between devices  2.87 us (2%)
    pallas_call x1, Pallas kernels, attention(): pl.pallas_call(kernel, grid=(ways, tiles), out_shape=(jax.ShapeDtypeStruc...  52.5 us
    pallas_call x1, Pallas kernels, spread(): pl.pallas_call(lambda *refs: spread_kernel(ways, group, *refs), out_shape...  49.2 us
    ppermute x1, waiting for transfers between devices, per_device(): lax.ppermute(tokens, 'tp', [(i, (i - d) % tp) for i in range(tp)])  17.4 us
    pallas_call x1, Pallas kernels, collect(): pl.pallas_call(lambda *refs: collect_kernel(ways, group, tp, *refs), out_...  13.5 us
    dot_general x3, matrix products, turned(): lax.dot_general(matrix, normed, (((0,), (1,)), ((), ())), preferred_eleme...  6.94 us
    dot_general x1, matrix products, per_device(): jnp.dot(merged, output_weight, preferred_element_type=jnp.float32)  6.7 us
    reduce_sum x1, other arithmetic, per_device(): jnp.sum(convolved, axis=1)  5.05 us
    unnamed x91, local copies, waits for them, and re-layouts  4.18 us
  transfers between devices with their start and end apart: 2, of which 1 were waited for; matrix products, arithmetic and copies ran while one was open for 12% of the time, Pallas kernels for 54%

profile of v1, /device:TPU:29, one launch (start us, length us, event | category | flops | bytes accessed | tf_op | source)
XLA Modules:
  0.0 188.3 jit_solution(14547395179149964262)
XLA Ops:
  0.6 0.0 copy-start
  0.6 1.3 collective-permute-start
  1.9 0.8 copy.24.gain_ref
  2.7 1.3 dynamic_slice.3.lam_ref
  4.0 1.6 fusion.56
  5.6 1.8 fusion.55
  7.4 0.3 multiply_cosine_fusion
  7.7 17.4 %collective-permute-done = bf16[256,2048]{1,0:T(8,128)(2,1)} collective-permute-done((bf16[256,2048]{1,0:T(8,128)(2,1)}, bf16[256,2048]{1,0:T(8,128)(2,1)}, u32[]{:S(2)}, u32[]{:S(2)}) %collective-permute-start) | collective-permute-done | bytes 1048608 | tf_op jit(solution)/shard_map/ppermute | solution.py:352
  25.1 1.7 broadcast_select_fusion.1
  26.8 0.0 copy-start.4
  26.8 0.0 copy-start.41
  26.8 0.0 copy-start.44
  26.8 0.5 fusion
  27.3 1.5 copy-done.41
  28.7 1.5 fusion.7
  30.2 0.1 copy-done.42
  30.3 1.3 fusion.12
  31.7 0.8 copy-done.7
  32.4 1.6 collective-permute-start.1
  34.1 1.4 multiply_reduce_fusion.2
  35.5 0.0 copy-start.40
  35.5 1.5 multiply_reduce_fusion.1
  37.0 0.5 multiply_multiply_fusion
  37.5 1.1 subtract_convert_fusion
  38.6 0.8 pad_maximum_fusion.2
  39.4 2.0 %copy.22 = bf16[4,128,512]{1,2,0:T(8,128)(2,1)} copy(bf16[4,128,512]{2,1,0:T(8,128)(2,1)} %bitcast.69) | data formatting | bytes 1048576 | tf_op jit(solution)/shard_map/convert_element_type | solution.py:323
  41.5 4.1 %fusion.13 = bf16[512,512]{0,1:T(8,128)(2,1)} fusion(bf16[2048,512]{1,0:T(8,128)(2,1)} %param.18, f32[2048]{0:T(1024)} %param.15, f32[512]{0:T(512)} %copy-done.39, bf16[256,2048]{1,0:T(8,128)(2,1)} %copy-done.4, bf16[256,2048]{1,0:T(8,128)(2,1)S(1)} %get-tuple-element.25), kind=kOutput, calls=%fused_computation.22 | convolution fusion | flops 1081344000 | bytes 4728832 | tf_op jit(solution)/shard_map/dot_general | solution.py:363
  45.5 1.2 reshape_reshape.3
  46.8 1.1 copy.23
  47.9 2.1 %pad_maximum_fusion.1.refs_1_ = bf16[4,1024,128]{2,1,0:T(8,128)(2,1)} fusion(bf16[4,512,128]{2,1,0:T(8,128)(2,1)} %bitcast.71, bf16[4,512,128]{2,1,0:T(8,128)(2,1)S(1)} %bitcast.70), kind=kLoop, calls=%fused_computation.84 | loop fusion | flops 2097152 | bytes 2097152 | tf_op jit(solution)/shard_map/concatenate | solution.py:378
  50.0 0.9 maximum_multiply_fusion
  51.0 49.2 %spread.1 = (bf16[4,128,512]{2,1,0:T(8,128)(2,1)}, bf16[16,1024,128]{2,1,0:T(8,128)(2,1)}) custom-call(bf16[4,128,512]{2,1,0:T(8,128)(2,1)} %bitcast.68, bf16[4,1024,128]{2,1,0:T(8,128)(2,1)} %pad_maximum_fusion.1.refs_1_), custom_call_target="tpu_custom_call" | custom-call | tf_op jit(solution)/shard_map/spread/pallas_call | solution.py:122
  100.2 1.0 copy-done.2
  101.5 52.5 %attend.1 = (bf16[4,512,128]{2,1,0:T(8,128)(2,1)S(1)}, f32[4,2,512]{2,1,0:T(2,128)S(1)}) custom-call(s32[1]{0:T(128)} %bitcast.place_ref, f32[1]{0:T(128)} %dynamic_slice.3.lam_ref, f32[128,1]{1,0:T(8,128)S(1)} %copy.24.gain_ref, bf16[4,128,512]{2,1,0:T(8,128)(2,1)S(1)} %copy-done.2, bf16[16,1024,128]{2,1,0:T(8,128)(2,1)} %get-tuple-element.10.kv_ref), custom_call_target="tpu_custom_call" | custom-call | tf_op jit(solution)/shard_map/attend/pallas_call | solution.py:293
  154.1 0.0 copy-start.1
  154.1 0.0 copy-start.3
  154.1 0.0 collective-permute-done.1
  154.1 0.2 maximum_convert_fusion
  154.5 0.0 copy-start.37
  154.6 0.0 copy-start.38
  154.6 5.1 %fusion.53 = (f32[512]{0:T(512)S(1)}, f32[512]{0:T(512)S(1)}, f32[512,512]{1,0:T(8,128)S(1)}) fusion(f32[542,512]{1,0:T(8,128)S(1)} %maximum_convert_fusion, f32[512]{0:T(512)S(1)} %bitcast.87, f32[512]{0:T(512)S(1)} %bitcast.88, f32[512]{0:T(512)S(1)} %bitcast.90, f32[512]{0:T(512)S(1)} %bitcast.91, f32[512]{0:T(512)S(1)} %bitcast.92, f32[512]{0:T(512)S(1)} %bitcast.93, ...), kind=kLoop, calls=%fused_computation.113 | loop fusion | flops 16776192 | bytes 33622016 | tf_op jit(solution)/shard_map/reduce_sum | solution.py:389
  159.6 4.0 %all-reduce = (f32[512]{0:T(512)S(1)}, f32[512]{0:T(512)S(1)}) all-reduce(f32[512]{0:T(512)S(1)} %get-tuple-element.21, f32[512]{0:T(512)S(1)} %get-tuple-element.20), channel_id=1, replica_groups=mesh['sp'=16,'tp'=2] {'tp'}, use_global_device_ids=true, to_apply=%region_6.7 | all-reduce | flops 1024 | bytes 8192 | tf_op jit(solution)/shard_map/psum | solution.py:388
  163.7 1.2 multiply_convert_fusion
  164.9 13.5 %collect.1 = (bf16[8,256,128]{2,1,0:T(8,128)(2,1)}, f32[4,2,512]{2,1,0:T(2,128)}, bf16[2,256,512]{2,1,0:T(8,128)(2,1)}) custom-call(bf16[4,2,256,128]{3,2,1,0:T(8,128)(2,1)} %bitcast.66, f32[4,2,512]{2,1,0:T(2,128)} %copy-done.3, bf16[2,256,512]{2,1,0:T(8,128)(2,1)} %bitcast.67), custom_call_target="tpu_custom_call" | custom-call | tf_op jit(solution)/shard_map/collect/pallas_call | solution.py:223
  178.4 1.3 copy.25
  179.7 1.2 copy.26
  180.9 0.6 copy.27
  181.6 6.7 %convolution_convert_fusion = bf16[256,2048]{1,0:T(8,128)(2,1)} fusion(bf16[2048,2048]{1,0:T(8,128)(2,1)} %param.27, bf16[256,1024]{0,1:T(8,128)(2,1)S(1)} %bitcast.75, bf16[256,1024]{0,1:T(8,128)(2,1)S(1)} %bitcast.74), kind=kOutput, calls=%fused_computation.5 | convolution fusion | flops 2150105088 | bytes 10485760 | tf_op jit(solution)/shard_map/dot_general | solution.py:407
  (83 shorter events, 0.2 us)
Async XLA Ops:
  0.6 33.4 %copy-start = (bf16[2048,512]{1,0:T(8,128)(2,1)S(1)}, bf16[2048,512]{1,0:T(8,128)(2,1)}, u32[]{:S(2)}) copy-start(bf16[2048,512]{1,0:T(8,128)(2,1)} %param.16) | copy-start | bytes 6291460
  0.6 24.4 %collective-permute-start = (bf16[256,2048]{1,0:T(8,128)(2,1)}, bf16[256,2048]{1,0:T(8,128)(2,1)}, u32[]{:S(2)}, u32[]{:S(2)}) collective-permute-start(bf16[256,2048]{1,0:T(8,128)(2,1)} %param.14), channel_id=1, source_target_pairs={{0,1},{1,0},{2,3},{3,2},{4,5},{5,4},{6,7},{7,6},{8,9},{9,8},{10,11... | collective-permute-start | bytes 3145736 | tf_op jit(solution)/shard_map/ppermute | solution.py:352
  26.8 8.7 %copy-start.4 = (bf16[256,2048]{1,0:T(8,128)(2,1)}, bf16[256,2048]{1,0:T(8,128)(2,1)S(1)}, u32[]{:S(2)}) copy-start(bf16[256,2048]{1,0:T(8,128)(2,1)S(1)} %get-tuple-element.26) | copy-start | bytes 3145732
  26.8 2.0 %copy-start.41 = (bf16[2048,512]{1,0:T(8,128)(2,1)S(1)}, bf16[2048,512]{1,0:T(8,128)(2,1)}, u32[]{:S(2)}) copy-start(bf16[2048,512]{1,0:T(8,128)(2,1)} %param.20) | copy-start | bytes 6291460
  26.8 2.0 %copy-start.44 = (f32[2048]{0:T(1024)S(1)}, f32[2048]{0:T(1024)}, u32[]{:S(2)}) copy-start(f32[2048]{0:T(1024)} %param.15) | copy-start | bytes 24580
  28.7 6.8 %copy-start.39 = (f32[512]{0:T(512)}, f32[512]{0:T(512)S(1)}, u32[]{:S(2)}) copy-start(f32[512]{0:T(512)S(1)} %add_rsqrt_fusion.3) | copy-start | bytes 6148
  28.7 1.6 copy-start.42
  31.6 0.8 copy-start.7
  32.4 3.1 %copy-start.43 = (bf16[2048,512]{1,0:T(8,128)(2,1)S(1)}, bf16[2048,512]{1,0:T(8,128)(2,1)}, u32[]{:S(2)}) copy-start(bf16[2048,512]{1,0:T(8,128)(2,1)} %param.17) | copy-start | bytes 6291460
  32.4 121.6 %collective-permute-start.1 = (bf16[30,512]{1,0:T(8,128)(2,1)S(1)}, bf16[30,512]{1,0:T(8,128)(2,1)S(1)}, u32[]{:S(2)}, u32[]{:S(2)}) collective-permute-start(bf16[30,512]{1,0:T(8,128)(2,1)S(1)} %slice.272), channel_id=1, source_target_pairs={{0,2},{2,4},{4,6},{6,8},{8,10},{10,12},{12,14},{14,16},{16,18},{18... | collective-permute-start | bytes 92168 | tf_op jit(solution)/shard_map/ppermute | solution.py:17
  35.5 1.5 copy-start.40
  45.5 2.4 %copy-start.5 = (bf16[4,128,512]{1,2,0:T(8,128)(2,1)S(1)}, bf16[4,128,512]{1,2,0:T(8,128)(2,1)}, u32[]{:S(2)}) copy-start(bf16[4,128,512]{1,2,0:T(8,128)(2,1)} %copy.22) | copy-start | bytes 1572868
  47.9 2.1 %copy-start.6 = (bf16[4,2,32,512]{3,2,1,0:T(8,128)(2,1)S(1)}, bf16[4,2,32,512]{3,2,1,0:T(8,128)(2,1)}, u32[]{:S(2)}) copy-start(bf16[4,2,32,512]{3,2,1,0:T(8,128)(2,1)} %get-tuple-element.32) | copy-start | bytes 786436
  100.2 1.0 copy-start.2
  101.3 52.8 %copy-start.8 = (bf16[512,512]{1,0:T(8,128)(2,1)S(1)}, bf16[512,512]{1,0:T(8,128)(2,1)}, u32[]{:S(2)}) copy-start(bf16[512,512]{1,0:T(8,128)(2,1)} %copy-done.7) | copy-start | bytes 1572868
  101.3 53.0 %copy-start.10 = (f32[1,512]{1,0:T(1,128)S(1)}, f32[1,512]{1,0:T(1,128)}, u32[]{:S(2)}) copy-start(f32[1,512]{1,0:T(1,128)} %get-tuple-element.56) | copy-start | bytes 6148
  101.3 53.0 %copy-start.11 = (f32[1,512]{1,0:T(1,128)S(1)}, f32[1,512]{1,0:T(1,128)}, u32[]{:S(2)}) copy-start(f32[1,512]{1,0:T(1,128)} %get-tuple-element.57) | copy-start | bytes 6148
  101.3 53.0 %copy-start.12 = (f32[1,512]{1,0:T(1,128)S(1)}, f32[1,512]{1,0:T(1,128)}, u32[]{:S(2)}) copy-start(f32[1,512]{1,0:T(1,128)} %get-tuple-element.58) | copy-start | bytes 6148
  101.3 53.0 %copy-start.13 = (f32[1,512]{1,0:T(1,128)S(1)}, f32[1,512]{1,0:T(1,128)}, u32[]{:S(2)}) copy-start(f32[1,512]{1,0:T(1,128)} %get-tuple-element.59) | copy-start | bytes 6148
  101.3 53.0 %copy-start.14 = (f32[1,512]{1,0:T(1,128)S(1)}, f32[1,512]{1,0:T(1,128)}, u32[]{:S(2)}) copy-start(f32[1,512]{1,0:T(1,128)} %get-tuple-element.60) | copy-start | bytes 6148
  101.3 53.0 %copy-start.15 = (f32[1,512]{1,0:T(1,128)S(1)}, f32[1,512]{1,0:T(1,128)}, u32[]{:S(2)}) copy-start(f32[1,512]{1,0:T(1,128)} %get-tuple-element.61) | copy-start | bytes 6148
  101.3 53.0 %copy-start.16 = (f32[1,512]{1,0:T(1,128)S(1)}, f32[1,512]{1,0:T(1,128)}, u32[]{:S(2)}) copy-start(f32[1,512]{1,0:T(1,128)} %get-tuple-element.62) | copy-start | bytes 6148
  101.3 53.0 %copy-start.17 = (f32[1,512]{1,0:T(1,128)S(1)}, f32[1,512]{1,0:T(1,128)}, u32[]{:S(2)}) copy-start(f32[1,512]{1,0:T(1,128)} %get-tuple-element.63) | copy-start | bytes 6148
  101.3 53.0 %copy-start.18 = (f32[1,512]{1,0:T(1,128)S(1)}, f32[1,512]{1,0:T(1,128)}, u32[]{:S(2)}) copy-start(f32[1,512]{1,0:T(1,128)} %get-tuple-element.33) | copy-start | bytes 6148
  101.3 53.0 %copy-start.19 = (f32[1,512]{1,0:T(1,128)S(1)}, f32[1,512]{1,0:T(1,128)}, u32[]{:S(2)}) copy-start(f32[1,512]{1,0:T(1,128)} %get-tuple-element.34) | copy-start | bytes 6148
  101.4 53.0 %copy-start.20 = (f32[1,512]{1,0:T(1,128)S(1)}, f32[1,512]{1,0:T(1,128)}, u32[]{:S(2)}) copy-start(f32[1,512]{1,0:T(1,128)} %get-tuple-element.35) | copy-start | bytes 6148
  101.4 53.0 %copy-start.21 = (f32[1,512]{1,0:T(1,128)S(1)}, f32[1,512]{1,0:T(1,128)}, u32[]{:S(2)}) copy-start(f32[1,512]{1,0:T(1,128)} %get-tuple-element.36) | copy-start | bytes 6148
  101.4 53.0 %copy-start.22 = (f32[1,512]{1,0:T(1,128)S(1)}, f32[1,512]{1,0:T(1,128)}, u32[]{:S(2)}) copy-start(f32[1,512]{1,0:T(1,128)} %get-tuple-element.37) | copy-start | bytes 6148
  101.4 53.0 %copy-start.23 = (f32[1,512]{1,0:T(1,128)S(1)}, f32[1,512]{1,0:T(1,128)}, u32[]{:S(2)}) copy-start(f32[1,512]{1,0:T(1,128)} %get-tuple-element.38) | copy-start | bytes 6148
  101.4 53.0 %copy-start.24 = (f32[1,512]{1,0:T(1,128)S(1)}, f32[1,512]{1,0:T(1,128)}, u32[]{:S(2)}) copy-start(f32[1,512]{1,0:T(1,128)} %get-tuple-element.39) | copy-start | bytes 6148
  101.4 53.0 %copy-start.25 = (f32[1,512]{1,0:T(1,128)S(1)}, f32[1,512]{1,0:T(1,128)}, u32[]{:S(2)}) copy-start(f32[1,512]{1,0:T(1,128)} %get-tuple-element.40) | copy-start | bytes 6148
  101.4 53.0 %copy-start.26 = (f32[1,512]{1,0:T(1,128)S(1)}, f32[1,512]{1,0:T(1,128)}, u32[]{:S(2)}) copy-start(f32[1,512]{1,0:T(1,128)} %get-tuple-element.41) | copy-start | bytes 6148
  101.4 53.0 %copy-start.27 = (f32[1,512]{1,0:T(1,128)S(1)}, f32[1,512]{1,0:T(1,128)}, u32[]{:S(2)}) copy-start(f32[1,512]{1,0:T(1,128)} %get-tuple-element.42) | copy-start | bytes 6148
  101.4 53.0 %copy-start.28 = (f32[1,512]{1,0:T(1,128)S(1)}, f32[1,512]{1,0:T(1,128)}, u32[]{:S(2)}) copy-start(f32[1,512]{1,0:T(1,128)} %get-tuple-element.43) | copy-start | bytes 6148
  101.4 53.0 %copy-start.29 = (f32[1,512]{1,0:T(1,128)S(1)}, f32[1,512]{1,0:T(1,128)}, u32[]{:S(2)}) copy-start(f32[1,512]{1,0:T(1,128)} %get-tuple-element.44) | copy-start | bytes 6148
  101.5 53.0 %copy-start.30 = (f32[1,512]{1,0:T(1,128)S(1)}, f32[1,512]{1,0:T(1,128)}, u32[]{:S(2)}) copy-start(f32[1,512]{1,0:T(1,128)} %get-tuple-element.45) | copy-start | bytes 6148
  101.5 53.0 %copy-start.31 = (f32[1,512]{1,0:T(1,128)S(1)}, f32[1,512]{1,0:T(1,128)}, u32[]{:S(2)}) copy-start(f32[1,512]{1,0:T(1,128)} %get-tuple-element.46) | copy-start | bytes 6148
  101.5 53.0 %copy-start.32 = (f32[1,512]{1,0:T(1,128)S(1)}, f32[1,512]{1,0:T(1,128)}, u32[]{:S(2)}) copy-start(f32[1,512]{1,0:T(1,128)} %get-tuple-element.47) | copy-start | bytes 6148
  101.5 53.0 %copy-start.33 = (f32[1,512]{1,0:T(1,128)S(1)}, f32[1,512]{1,0:T(1,128)}, u32[]{:S(2)}) copy-start(f32[1,512]{1,0:T(1,128)} %get-tuple-element.48) | copy-start | bytes 6148
  101.5 53.0 %copy-start.34 = (f32[1,512]{1,0:T(1,128)S(1)}, f32[1,512]{1,0:T(1,128)}, u32[]{:S(2)}) copy-start(f32[1,512]{1,0:T(1,128)} %get-tuple-element.49) | copy-start | bytes 6148
  101.5 53.0 %copy-start.35 = (f32[1,512]{1,0:T(1,128)S(1)}, f32[1,512]{1,0:T(1,128)}, u32[]{:S(2)}) copy-start(f32[1,512]{1,0:T(1,128)} %get-tuple-element.50) | copy-start | bytes 6148
  101.5 53.0 %copy-start.36 = (f32[1,512]{1,0:T(1,128)S(1)}, f32[1,512]{1,0:T(1,128)}, u32[]{:S(2)}) copy-start(f32[1,512]{1,0:T(1,128)} %get-tuple-element.51) | copy-start | bytes 6148
  154.1 5.6 %copy-start.1 = (bf16[4,512,128]{2,1,0:T(8,128)(2,1)}, bf16[4,512,128]{2,1,0:T(8,128)(2,1)S(1)}, u32[]{:S(2)}) copy-start(bf16[4,512,128]{2,1,0:T(8,128)(2,1)S(1)} %get-tuple-element.11) | copy-start | bytes 1572868
  154.1 5.6 %copy-start.3 = (f32[4,2,512]{2,1,0:T(2,128)}, f32[4,2,512]{2,1,0:T(2,128)S(1)}, u32[]{:S(2)}) copy-start(f32[4,2,512]{2,1,0:T(2,128)S(1)} %get-tuple-element.12.refs_1_) | copy-start | bytes 49156
  154.5 9.1 %copy-start.37 = (f32[512]{0:T(512)S(1)}, f32[512]{0:T(512)}, u32[]{:S(2)}) copy-start(f32[512]{0:T(512)} %param.26) | copy-start | bytes 6148
  154.6 9.1 %copy-start.38 = (f32[512]{0:T(512)S(1)}, f32[512]{0:T(512)}, u32[]{:S(2)}) copy-start(f32[512]{0:T(512)} %param.25) | copy-start | bytes 6148
  178.4 2.5 %copy-start.9 = (f32[4,2,512]{2,1,0:T(2,128)S(1)}, f32[4,2,512]{2,1,0:T(2,128)}, u32[]{:S(2)}) copy-start(f32[4,2,512]{2,1,0:T(2,128)} %get-tuple-element.15) | copy-start | bytes 49156

commit v2 on v1

--- a/solution.py
+++ b/solution.py
@@ -15,6 +15,12 @@
     count = lax.axis_size(axis)
     leading, last = (max(0, -steps), min(count, count - steps))
     return lax.ppermute(value, axis, [(source, source + steps) for source in range(leading, last)])
+
+
+def flipped(g, a, group):
+    if group % 2:
+        return g
+    return jnp.where(a % 2 == 0, g, group - 1 - g)
 
 
 def spread_kernel(ways, group, q_ref, kv_ref, qo_ref, kvo_ref, qsend, qrecv, ksend, kfwd, krelay, krecv, local):
@@ -32,6 +38,7 @@
     peers += [a * group + same(d) for d in range(1, half)]
     if cores == 2:
         peers.append(mate)
+        peers += [lax.rem(a + d, ways) * group + group - 1 - g for d in range(ways)]
     barrier = pltpu.get_barrier_semaphore()
     for peer in peers:
         pl.semaphore_signal(barrier, inc=1, device_id={"sp": peer}, device_id_type=MESH)
@@ -43,12 +50,20 @@
             device_id={"sp": peer}, device_id_type=MESH)
 
     sends = []
-    locals_ = [
-        pltpu.make_async_copy(kv_ref.at[a], kvo_ref.at[me], local.at[0]),
-        pltpu.make_async_copy(q_ref.at[a], qo_ref.at[a], local.at[1]),
-    ]
-    for c in locals_:
-        c.start()
+    keep = pltpu.make_async_copy(kv_ref.at[a], kvo_ref.at[me], local.at[0])
+    keep_q = pltpu.make_async_copy(q_ref.at[a], qo_ref.at[a], local.at[1])
+    keep.start()
+
+    def q_copy(h, slot, d):
+        return pltpu.make_async_remote_copy(
+            src_ref=q_ref.at[h], dst_ref=qo_ref.at[slot], send_sem=qsend.at[d], recv_sem=qrecv.at[slot],
+            device_id={"sp": h * group + flipped(g, a, group)}, device_id_type=MESH)
+
+    stays = a % 2 == 0 if cores == 2 else a >= 0
+
+    @pl.when(stays)
+    def _():
+        keep_q.start()
     order = list(range(1, ways))
     for d in order:
         h = lax.rem(a + d, ways)
@@ -87,12 +102,13 @@
 
     forward(0)
     for d in order:
-        h = lax.rem(a + d, ways)
-        c = pltpu.make_async_remote_copy(
-            src_ref=q_ref.at[h], dst_ref=qo_ref.at[a], send_sem=qsend.at[d - 1], recv_sem=qrecv.at[a],
-            device_id={"sp": h * group + g}, device_id_type=MESH)
+        c = q_copy(lax.rem(a + d, ways), a, d)
         c.start()
         sends.append(c)
+    if cores == 2:
+        @pl.when(jnp.logical_not(stays))
+        def _():
+            q_copy(a, a, 0).start()
     for d in range(1, ways):
         forward(d)
         relay(d - 1)
@@ -105,13 +121,19 @@
                 kv_copy(kvo_ref.at[slot], slot, krelay.at[0, 0], mate).wait_recv()
     for d in range(1, ways):
         src_a = lax.rem(a + ways - d, ways)
-        pltpu.make_async_remote_copy(
-            src_ref=q_ref.at[a], dst_ref=qo_ref.at[src_a], send_sem=qsend.at[d - 1],
-            recv_sem=qrecv.at[src_a], device_id={"sp": me}, device_id_type=MESH).wait_recv()
+        q_copy(a, src_a, d).wait_recv()
     for c in sends:
         c.wait_send()
-    for c in locals_:
-        c.wait()
+    keep.wait()
+
+    @pl.when(stays)
+    def _():
+        keep_q.wait()
+
+    if cores == 2:
+        @pl.when(jnp.logical_not(stays))
+        def _():
+            q_copy(a, a, 0).wait()
 
 
 def spread(q, kv, ways, group):
@@ -128,7 +150,7 @@
         in_specs=[any_, any_],
         out_specs=(any_, any_),
         scratch_shapes=[
-            pltpu.SemaphoreType.DMA((n,)),
+            pltpu.SemaphoreType.DMA((ways,)),
             pltpu.SemaphoreType.DMA((ways,)),
             pltpu.SemaphoreType.DMA((n,)),
             pltpu.SemaphoreType.DMA((ways, half)),
@@ -154,20 +176,35 @@
         return lax.rem(a + da, ways), lax.rem(t + dt, tp)
 
     total = ways * tp
+    both = group % 2 == 0
     barrier = pltpu.get_barrier_semaphore()
-    for i in range(1, total):
+    for i in range(total):
         pa, pt = coords(i)
-        pl.semaphore_signal(barrier, inc=1, device_id={"sp": pa * group + g, "tp": pt}, device_id_type=MESH)
-    pl.semaphore_wait(barrier, total - 1)
+        if i:
+            pl.semaphore_signal(barrier, inc=1, device_id={"sp": pa * group + g, "tp": pt}, device_id_type=MESH)
+        if both:
+            pl.semaphore_signal(
+                barrier, inc=1, device_id={"sp": pa * group + group - 1 - g, "tp": pt}, device_id_type=MESH)
+    pl.semaphore_wait(barrier, 2 * total - 1 if both else total - 1)
 
     head = t * ways + a
+
+    def att_copy(i, slot):
+        pa, pt = coords(i)
+        return pltpu.make_async_remote_copy(
+            src_ref=att_ref.at[pa, pt], dst_ref=ao_ref.at[slot], send_sem=asend.at[i], recv_sem=arecv.at[slot],
+            device_id={"sp": pa * group + flipped(g, pa, group), "tp": pt}, device_id_type=MESH)
+
+    def lt_copy(i, slot):
+        pa = lax.rem(a + i, ways)
+        return pltpu.make_async_remote_copy(
+            src_ref=lt_ref.at[pa], dst_ref=lo_ref.at[slot], send_sem=lsend.at[i], recv_sem=lrecv.at[slot],
+            device_id={"sp": pa * group + flipped(g, pa, group), "tp": t}, device_id_type=MESH)
+
+    stays = a % 2 == 0 if both else a >= 0
     sends = []
-    for i in list(range(total - 1, 0, -1)):
-        pa, pt = coords(i)
-        dev = {"sp": pa * group + g, "tp": pt}
-        c = pltpu.make_async_remote_copy(
-            src_ref=att_ref.at[pa, pt], dst_ref=ao_ref.at[head],
-            send_sem=asend.at[i], recv_sem=arecv.at[head], device_id=dev, device_id_type=MESH)
+    for i in range(total - 1, 0, -1):
+        c = att_copy(i, head)
         c.start()
         sends.append(c)
     for i in range(1, tp):
@@ -179,41 +216,51 @@
         c.start()
         sends.append(c)
     for i in range(1, ways):
-        pa = lax.rem(a + i, ways)
-        c = pltpu.make_async_remote_copy(
-            src_ref=lt_ref.at[pa], dst_ref=lo_ref.at[a], send_sem=lsend.at[i], recv_sem=lrecv.at[a],
-            device_id={"sp": pa * group + g, "tp": t}, device_id_type=MESH)
+        c = lt_copy(i, a)
         c.start()
         sends.append(c)
+    keep = pltpu.make_async_copy(conv_ref.at[t], co_ref.at[t], local.at[1])
+    keep.start()
     mine = [
         pltpu.make_async_copy(att_ref.at[a, t], ao_ref.at[head], local.at[0]),
-        pltpu.make_async_copy(conv_ref.at[t], co_ref.at[t], local.at[1]),
         pltpu.make_async_copy(lt_ref.at[a], lo_ref.at[a], local.at[2]),
     ]
-    for c in mine:
-        c.start()
+
+    @pl.when(stays)
+    def _():
+        for c in mine:
+            c.start()
+
+    if both:
+        @pl.when(jnp.logical_not(stays))
+        def _():
+            att_copy(0, head).start()
+            lt_copy(0, a).start()
     for i in range(1, total):
         pa, pt = coords(i)
-        h = pt * ways + pa
-        pltpu.make_async_remote_copy(
-            src_ref=att_ref.at[a, t], dst_ref=ao_ref.at[h],
-            send_sem=asend.at[i], recv_sem=arecv.at[h],
-            device_id={"sp": me, "tp": t}, device_id_type=MESH).wait_recv()
+        att_copy(i, pt * ways + pa).wait_recv()
     for i in range(1, tp):
         pa, pt = coords(i)
         pltpu.make_async_remote_copy(
             src_ref=conv_ref.at[t], dst_ref=co_ref.at[pt],
             send_sem=csend.at[i], recv_sem=crecv.at[pt],
-            device_id={"sp": me, "tp": t}, device_id_type=MESH).wait_recv()
+            device_id={"sp": me, "tp": pt}, device_id_type=MESH).wait_recv()
     for i in range(1, ways):
-        pa = lax.rem(a + i, ways)
-        pltpu.make_async_remote_copy(
-            src_ref=lt_ref.at[a], dst_ref=lo_ref.at[pa], send_sem=lsend.at[i], recv_sem=lrecv.at[pa],
-            device_id={"sp": me, "tp": t}, device_id_type=MESH).wait_recv()
+        lt_copy(i, lax.rem(a + i, ways)).wait_recv()
     for c in sends:
         c.wait_send()
-    for c in mine:
-        c.wait()
+    keep.wait()
+
+    @pl.when(stays)
+    def _():
+        for c in mine:
+            c.wait()
+
+    if both:
+        @pl.when(jnp.logical_not(stays))
+        def _():
+            att_copy(0, head).wait()
+            lt_copy(0, a).wait()
 
 
 def collect(att, lt, conv, ways, group, tp):
@@ -249,67 +296,60 @@
     blocks = kv.shape[0]
     vdim = head_gain.shape[0]
     group = blocks // ways
-    tile = min(tile, rows)
+    tile = math.gcd(tile, rows)
     tiles = rows // tile
-
-    def kernel(place_ref, lam_ref, gain_ref, q_ref, kv_ref, o_ref, lt_ref):
-        i = pl.program_id(0)
-        s = pl.program_id(1)
-        chunk = i * group + place_ref[0]
+    def kernel(place_ref, lam_ref, gain_ref, q_ref, kv_ref, o_ref, lt_ref, sa, sb, acc_ref):
+        i = pl.program_id(0); s = pl.program_id(1)
+        chunk = i * group + flipped(place_ref[0], i, group)
         qs = [q_ref[0, m * hd:(m + 1) * hd, :] for m in range(2)]
-
-        def step(j, carry, masked):
-            out = []
-            kb = kv_ref[j, :rows]
-            vb = jnp.concatenate(
-                [kv_ref[j, rows + b * vdim:rows + (b + 1) * vdim] for b in range(rows // 128)], axis=1)
+        def score(j, ref):
             for m in range(2):
-                top, tot, acc = carry[m]
-                sc = jnp.dot(kb[:, m * hd:(m + 1) * hd], qs[m], preferred_element_type=jnp.float32)
+                ref[m] = jnp.dot(kv_ref[j, :rows, m * hd:(m + 1) * hd], qs[m], preferred_element_type=jnp.float32)
+        def absorb(j, ref, tops, masked=False):
+            vb = jnp.concatenate([kv_ref[j, rows + b * vdim:rows + (b + 1) * vdim] for b in range(rows // 128)], axis=1)
+            vb = jnp.concatenate([vb, jnp.ones((16, rows), jnp.bfloat16)], axis=0)
+            out=[]
+            for m in range(2):
+                sc = ref[m]
                 if masked:
                     kp = lax.broadcasted_iota(jnp.int32, sc.shape, 0)
                     qp = lax.broadcasted_iota(jnp.int32, sc.shape, 1) + s * tile
                     sc = jnp.where(kp <= qp, sc, NEG)
-                new = jnp.maximum(top, jnp.max(sc, axis=0, keepdims=True))
+                new = jnp.maximum(tops[m], jnp.max(sc, axis=0, keepdims=True))
                 p = jnp.exp(sc - new)
-                f = jnp.exp(top - new)
-                tot = tot * f + jnp.sum(p, axis=0, keepdims=True)
-                acc = acc * f + jnp.dot(vb, p.astype(jnp.bfloat16), preferred_element_type=jnp.float32)
-                out.append((new, tot, acc))
+                f = jnp.exp(tops[m] - new)
+                acc_ref[m] = acc_ref[m] * f + jnp.dot(vb, p.astype(jnp.bfloat16), preferred_element_type=jnp.float32)
+                out.append(new)
             return tuple(out)
-
-        one = (jnp.full((1, tile), NEG, jnp.float32), jnp.zeros((1, tile), jnp.float32),
-               jnp.zeros((vdim, tile), jnp.float32))
-        carry = step(chunk, (one, one), True)
-        carry = lax.fori_loop(0, chunk, lambda j, c: step(j, c, False), carry)
-        (t0, l0, a0), (t1, l1, a1) = carry
+        acc_ref[...] = jnp.zeros_like(acc_ref)
+        one = jnp.full((1, tile), NEG, jnp.float32)
+        score(chunk, sa)
+        score(0, sb)
+        tops = absorb(chunk, sa, (one, one), True)
+
+        def pair(j, tops):
+            score(2 * j + 1, sa)
+            tops = absorb(2 * j, sb, tops)
+            score(2 * j + 2, sb)
+            return absorb(2 * j + 1, sa, tops)
+
+        tops = lax.fori_loop(0, chunk // 2, pair, tops)
+        tops = lax.cond(chunk % 2 == 1, lambda t: absorb(chunk - 1, sb, t), lambda t: t, tops)
+        a0=acc_ref[0]; a1=acc_ref[1]
+        t0,t1=tops
+        l0=a0[vdim:vdim+1]; l1=a1[vdim:vdim+1]; a0=a0[:vdim]; a1=a1[:vdim]
         heads = a0 / l0 - lam_ref[0] * a1 / l1
         heads = heads * lax.rsqrt(jnp.mean(heads * heads, axis=0, keepdims=True) + 1e-06) * gain_ref[...]
         o_ref[0] = heads.T.astype(jnp.bfloat16)
         lt_ref[0, 0:1, :] = t0 + jnp.log(l0)
         lt_ref[0, 1:2, :] = t1 + jnp.log(l1)
-
     smem = pl.BlockSpec(memory_space=pltpu.SMEM)
-    return pl.pallas_call(
-        kernel,
-        grid=(ways, tiles),
-        out_shape=(
-            jax.ShapeDtypeStruct((ways, rows, vdim), jnp.bfloat16),
-            jax.ShapeDtypeStruct((ways, 2, rows), jnp.float32),
-        ),
-        in_specs=[
-            smem, smem,
-            pl.BlockSpec((vdim, 1), lambda i, s: (0, 0)),
-            pl.BlockSpec((1, qdim, tile), lambda i, s: (i, 0, s)),
-            pl.BlockSpec(kv.shape, lambda i, s: (0, 0, 0)),
-        ],
-        out_specs=(
-            pl.BlockSpec((1, tile, vdim), lambda i, s: (i, s, 0)),
-            pl.BlockSpec((1, 2, tile), lambda i, s: (i, 0, s)),
-        ),
-        compiler_params=pltpu.CompilerParams(vmem_limit_bytes=50 << 20),
-        name="attend",
-    )(place, lam, head_gain.reshape(-1, 1), qt, kv)
+    return pl.pallas_call(kernel, grid=(ways, tiles),
+        out_shape=(jax.ShapeDtypeStruct((ways, rows, vdim), jnp.bfloat16), jax.ShapeDtypeStruct((ways, 2, rows), jnp.float32)),
+        in_specs=[smem, smem, pl.BlockSpec((vdim, 1), lambda i, s: (0, 0)), pl.BlockSpec((1, qdim, tile), lambda i, s: (i, 0, s)), pl.BlockSpec(kv.shape, lambda i, s: (0, 0, 0))],
+        out_specs=(pl.BlockSpec((1, tile, vdim), lambda i, s: (i, s, 0)), pl.BlockSpec((1, 2, tile), lambda i, s: (i, 0, s))),
+        scratch_shapes=[pltpu.VMEM((2,rows,tile),jnp.float32),pltpu.VMEM((2,rows,tile),jnp.float32),pltpu.VMEM((2,vdim+16,tile),jnp.float32)],
+        compiler_params=pltpu.CompilerParams(vmem_limit_bytes=58 << 20), name="attend")(place, lam, head_gain.reshape(-1, 1), qt, kv)
 
 
 def prepare_t(raw, qk_gain, cosine, sine):

time: 191 us -> 172 us (0.901)
  the two profiles are of different devices: /device:TPU:29 before, /device:TPU:11 now
where the time goes in v2:
time: 172 us; the launch traced here: 171 us
  Pallas kernels  96.7 us (56%)
  waiting for transfers between devices  18.2 us (11%)
  matrix products  16.4 us (10%)
  local copies, waits for them, and re-layouts  15.6 us (9%)
  other arithmetic  14.3 us (8%)
  starting transfers between devices  5.19 us (3%)
  blocking collectives  4.01 us (2%)
    pallas_call x1, Pallas kernels, spread(): pl.pallas_call(lambda *refs: spread_kernel(ways, group, *refs), out_shape...  40.7 us
    pallas_call x1, Pallas kernels, collect(): pl.pallas_call(lambda *refs: collect_kernel(ways, group, tp, *refs), out_...  29.4 us
    pallas_call x1, Pallas kernels, attention(): pl.pallas_call(kernel, grid=(ways, tiles), out_shape=(jax.ShapeDtypeStruc...  26.6 us
    ppermute x1, waiting for transfers between devices, per_device(): lax.ppermute(tokens, 'tp', [(i, (i - d) % tp) for i in range(tp)])  18.2 us
    dot_general x3, matrix products, turned(): lax.dot_general(matrix, normed, (((0,), (1,)), ((), ())), preferred_eleme...  6.93 us
    dot_general x1, matrix products, per_device(): jnp.dot(merged, output_weight, preferred_element_type=jnp.float32)  6.7 us
    reduce_sum x1, other arithmetic, per_device(): jnp.sum(convolved, axis=1)  5.05 us
    ppermute x1, starting transfers between devices, from_behind(): lax.ppermute(value, axis, [(source, source + steps) for source in range(l...  4.87 us
  transfers between devices with their start and end apart: 2, of which 1 were waited for; matrix products, arithmetic and copies ran while one was open for 13% of the time, Pallas kernels for 39%

profile of v2, /device:TPU:11, one launch (start us, length us, event | category | flops | bytes accessed | tf_op | source)
XLA Modules:
  0.0 171.5 jit_solution(7921875561589893534)
XLA Ops:
  0.6 0.0 copy-start
  0.6 0.3 collective-permute-start
  1.0 1.5 copy.24.gain_ref
  2.5 1.3 dynamic_slice.3.lam_ref
  3.8 1.0 fusion.56
  4.8 1.8 %fusion.55 = (f32[1,512]{1,0:T(1,128)S(1)}, f32[1,512]{1,0:T(1,128)S(1)}, f32[1,512]{1,0:T(1,128)S(1)}, f32[1,512]{1,0:T(1,128)S(1)}, f32[1,512]{1,0:T(1,128)S(1...) fusion(f32[31,512]{1,0:T(8,128)} %param.24), kind=kLoop, calls=%fused_computation.114 | loop fusion | bytes 77824 | tf_op jit(solution)/shard_map/slice | solution.py:427
  6.6 0.3 multiply_cosine_fusion
  6.9 18.2 %collective-permute-done = bf16[256,2048]{1,0:T(8,128)(2,1)} collective-permute-done((bf16[256,2048]{1,0:T(8,128)(2,1)}, bf16[256,2048]{1,0:T(8,128)(2,1)}, u32[]{:S(2)}, u32[]{:S(2)}) %collective-permute-start) | collective-permute-done | bytes 1048608 | tf_op jit(solution)/shard_map/ppermute | solution.py:392
  25.1 1.7 broadcast_select_fusion.1
  26.8 0.0 copy-start.1
  26.8 0.0 copy-start.22
  26.8 0.0 copy-start.25
  26.8 0.5 fusion
  27.3 1.5 copy-done.22
  28.7 0.0 copy-done.25
  28.7 1.5 fusion.7
  30.2 0.1 copy-done.23
  30.3 1.3 fusion.12
  31.6 0.0 copy-start.4
  31.7 0.8 copy-done.4
  32.4 4.9 %collective-permute-start.1 = (bf16[30,512]{1,0:T(8,128)(2,1)S(1)}, bf16[30,512]{1,0:T(8,128)(2,1)S(1)}, u32[]{:S(2)}, u32[]{:S(2)}) collective-permute-start(bf16[30,512]{1,0:T(8,128)(2,1)S(1)} %slice.272), channel_id=1, source_target_pairs={{0,2},{2,4},{4,6},{6,8},{8,10},{10,12},{12,14},{14,16},{16,18},{18... | collective-permute-start | bytes 92168 | tf_op jit(solution)/shard_map/ppermute | solution.py:17
  37.3 0.0 copy-done
  37.3 1.4 multiply_reduce_fusion.2
  38.8 0.0 copy-start.21
  38.8 1.5 multiply_reduce_fusion.1
  40.3 0.5 multiply_multiply_fusion
  40.8 1.1 subtract_convert_fusion
  41.9 0.8 pad_maximum_fusion.2
  42.7 2.0 %copy.22 = bf16[4,128,512]{1,2,0:T(8,128)(2,1)} copy(bf16[4,128,512]{2,1,0:T(8,128)(2,1)} %bitcast.68) | data formatting | bytes 1048576 | tf_op jit(solution)/shard_map/convert_element_type | solution.py:363
  44.7 4.0 %fusion.13 = bf16[512,512]{0,1:T(8,128)(2,1)} fusion(bf16[2048,512]{1,0:T(8,128)(2,1)} %param.18, f32[2048]{0:T(1024)} %param.15, f32[512]{0:T(512)} %copy-done.20, bf16[256,2048]{1,0:T(8,128)(2,1)} %copy-done.1, bf16[256,2048]{1,0:T(8,128)(2,1)S(1)} %get-tuple-element.25), kind=kOutput, calls=%fused_computation.22 | convolution fusion | flops 1081344000 | bytes 4728832 | tf_op jit(solution)/shard_map/dot_general | solution.py:403
  48.8 1.2 reshape_reshape.3
  50.0 1.1 copy.23
  51.1 2.1 %pad_maximum_fusion.1.refs_1_ = bf16[4,1024,128]{2,1,0:T(8,128)(2,1)} fusion(bf16[4,512,128]{2,1,0:T(8,128)(2,1)} %bitcast.70, bf16[4,512,128]{2,1,0:T(8,128)(2,1)S(1)} %bitcast.69), kind=kLoop, calls=%fused_computation.84 | loop fusion | flops 2097152 | bytes 2097152 | tf_op jit(solution)/shard_map/concatenate | solution.py:418
  53.3 0.9 maximum_multiply_fusion
  54.2 40.7 %spread.1 = (bf16[4,128,512]{2,1,0:T(8,128)(2,1)}, bf16[16,1024,128]{2,1,0:T(8,128)(2,1)}) custom-call(bf16[4,128,512]{2,1,0:T(8,128)(2,1)} %bitcast.67, bf16[4,1024,128]{2,1,0:T(8,128)(2,1)} %pad_maximum_fusion.1.refs_1_), custom_call_target="tpu_custom_call" | custom-call | tf_op jit(solution)/shard_map/spread/pallas_call | solution.py:144
  95.0 26.6 %attend.1 = (bf16[4,512,128]{2,1,0:T(8,128)(2,1)}, f32[4,2,512]{2,1,0:T(2,128)}) custom-call(s32[1]{0:T(128)} %bitcast.place_ref, f32[1]{0:T(128)} %dynamic_slice.3.lam_ref, f32[128,1]{1,0:T(8,128)} %copy.24.gain_ref, bf16[4,128,512]{2,1,0:T(8,128)(2,1)} %get-tuple-element.9.q_ref, bf16[16,1024,128]{2,1,0:T(8,128)(2,1)} %get-tuple-element.10.kv_ref), custom_call_target="tpu_custom_call" | custom-call | tf_op jit(solution)/shard_map/attend/pallas_call | solution.py:347
  121.6 0.0 collective-permute-done.1
  121.6 0.2 maximum_convert_fusion
  121.9 0.0 copy-start.18
  121.9 0.0 copy-start.19
  121.9 5.1 %fusion.53 = (f32[512]{0:T(512)S(1)}, f32[512]{0:T(512)S(1)}, f32[512,512]{1,0:T(8,128)S(1)}) fusion(f32[542,512]{1,0:T(8,128)S(1)} %maximum_convert_fusion, f32[512]{0:T(512)S(1)} %bitcast.87, f32[512]{0:T(512)S(1)} %bitcast.88, f32[512]{0:T(512)S(1)} %bitcast.90, f32[512]{0:T(512)S(1)} %bitcast.91, f32[512]{0:T(512)S(1)} %bitcast.92, f32[512]{0:T(512)S(1)} %bitcast.93, ...), kind=kLoop, calls=%fused_computation.113 | loop fusion | flops 16776192 | bytes 33622016 | tf_op jit(solution)/shard_map/reduce_sum | solution.py:429
  127.0 4.0 %all-reduce = (f32[512]{0:T(512)S(1)}, f32[512]{0:T(512)S(1)}) all-reduce(f32[512]{0:T(512)S(1)} %get-tuple-element.21, f32[512]{0:T(512)S(1)} %get-tuple-element.20), channel_id=1, replica_groups=mesh['sp'=16,'tp'=2] {'tp'}, use_global_device_ids=true, to_apply=%region_6.7 | all-reduce | flops 1024 | bytes 8192 | tf_op jit(solution)/shard_map/psum | solution.py:428
  131.0 1.2 multiply_convert_fusion
  132.2 29.4 %collect.1 = (bf16[8,256,128]{2,1,0:T(8,128)(2,1)}, f32[4,2,512]{2,1,0:T(2,128)}, bf16[2,256,512]{2,1,0:T(8,128)(2,1)}) custom-call(bf16[4,2,256,128]{3,2,1,0:T(8,128)(2,1)} %bitcast.71, f32[4,2,512]{2,1,0:T(2,128)} %get-tuple-element.12.refs_1_, bf16[2,256,512]{2,1,0:T(8,128)(2,1)} %bitcast.66), custom_call_target="tpu_custom_call" | custom-call | tf_op jit(solution)/shard_map/collect/pallas_call | solution.py:270
  161.7 1.3 copy.25
  162.9 1.2 copy.26
  164.2 0.6 copy.27
  164.8 6.7 %convolution_convert_fusion = bf16[256,2048]{1,0:T(8,128)(2,1)} fusion(bf16[2048,2048]{1,0:T(8,128)(2,1)} %param.27, bf16[256,1024]{0,1:T(8,128)(2,1)S(1)} %bitcast.75, bf16[256,1024]{0,1:T(8,128)(2,1)S(1)} %bitcast.74), kind=kOutput, calls=%fused_computation.5 | convolution fusion | flops 2150105088 | bytes 10485760 | tf_op jit(solution)/shard_map/dot_general | solution.py:447
  (45 shorter events, 0.2 us)
Async XLA Ops:
  0.6 36.7 %copy-start = (bf16[2048,512]{1,0:T(8,128)(2,1)S(1)}, bf16[2048,512]{1,0:T(8,128)(2,1)}, u32[]{:S(2)}) copy-start(bf16[2048,512]{1,0:T(8,128)(2,1)} %param.16) | copy-start | bytes 6291460
  0.6 24.4 %collective-permute-start = (bf16[256,2048]{1,0:T(8,128)(2,1)}, bf16[256,2048]{1,0:T(8,128)(2,1)}, u32[]{:S(2)}, u32[]{:S(2)}) collective-permute-start(bf16[256,2048]{1,0:T(8,128)(2,1)} %param.14), channel_id=1, source_target_pairs={{0,1},{1,0},{2,3},{3,2},{4,5},{5,4},{6,7},{7,6},{8,9},{9,8},{10,11... | collective-permute-start | bytes 3145736 | tf_op jit(solution)/shard_map/ppermute | solution.py:392
  26.8 12.0 %copy-start.1 = (bf16[256,2048]{1,0:T(8,128)(2,1)}, bf16[256,2048]{1,0:T(8,128)(2,1)S(1)}, u32[]{:S(2)}) copy-start(bf16[256,2048]{1,0:T(8,128)(2,1)S(1)} %get-tuple-element.26) | copy-start | bytes 3145732
  26.8 2.0 %copy-start.22 = (bf16[2048,512]{1,0:T(8,128)(2,1)S(1)}, bf16[2048,512]{1,0:T(8,128)(2,1)}, u32[]{:S(2)}) copy-start(bf16[2048,512]{1,0:T(8,128)(2,1)} %param.20) | copy-start | bytes 6291460
  26.8 2.0 %copy-start.25 = (f32[2048]{0:T(1024)S(1)}, f32[2048]{0:T(1024)}, u32[]{:S(2)}) copy-start(f32[2048]{0:T(1024)} %param.15) | copy-start | bytes 24580
  28.7 10.0 %copy-start.20 = (f32[512]{0:T(512)}, f32[512]{0:T(512)S(1)}, u32[]{:S(2)}) copy-start(f32[512]{0:T(512)S(1)} %add_rsqrt_fusion.3) | copy-start | bytes 6148
  28.7 1.6 copy-start.23
  31.6 0.8 copy-start.4
  32.4 6.3 %copy-start.24 = (bf16[2048,512]{1,0:T(8,128)(2,1)S(1)}, bf16[2048,512]{1,0:T(8,128)(2,1)}, u32[]{:S(2)}) copy-start(bf16[2048,512]{1,0:T(8,128)(2,1)} %param.17) | copy-start | bytes 6291460
  32.4 89.2 %collective-permute-start.1 = (bf16[30,512]{1,0:T(8,128)(2,1)S(1)}, bf16[30,512]{1,0:T(8,128)(2,1)S(1)}, u32[]{:S(2)}, u32[]{:S(2)}) collective-permute-start(bf16[30,512]{1,0:T(8,128)(2,1)S(1)} %slice.272), channel_id=1, source_target_pairs={{0,2},{2,4},{4,6},{6,8},{8,10},{10,12},{12,14},{14,16},{16,18},{18... | collective-permute-start | bytes 92168 | tf_op jit(solution)/shard_map/ppermute | solution.py:17
  38.8 1.5 copy-start.21
  48.8 2.4 %copy-start.2 = (bf16[4,128,512]{1,2,0:T(8,128)(2,1)S(1)}, bf16[4,128,512]{1,2,0:T(8,128)(2,1)}, u32[]{:S(2)}) copy-start(bf16[4,128,512]{1,2,0:T(8,128)(2,1)} %copy.22) | copy-start | bytes 1572868
  51.1 2.1 %copy-start.3 = (bf16[4,2,32,512]{3,2,1,0:T(8,128)(2,1)S(1)}, bf16[4,2,32,512]{3,2,1,0:T(8,128)(2,1)}, u32[]{:S(2)}) copy-start(bf16[4,2,32,512]{3,2,1,0:T(8,128)(2,1)} %get-tuple-element.32) | copy-start | bytes 786436
  94.9 26.7 %copy-start.5 = (bf16[512,512]{1,0:T(8,128)(2,1)S(1)}, bf16[512,512]{1,0:T(8,128)(2,1)}, u32[]{:S(2)}) copy-start(bf16[512,512]{1,0:T(8,128)(2,1)} %copy-done.4) | copy-start | bytes 1572868
  94.9 26.9 %copy-start.7 = (f32[1,512]{1,0:T(1,128)S(1)}, f32[1,512]{1,0:T(1,128)}, u32[]{:S(2)}) copy-start(f32[1,512]{1,0:T(1,128)} %get-tuple-element.41) | copy-start | bytes 6148
  94.9 26.9 %copy-start.8 = (f32[1,512]{1,0:T(1,128)S(1)}, f32[1,512]{1,0:T(1,128)}, u32[]{:S(2)}) copy-start(f32[1,512]{1,0:T(1,128)} %get-tuple-element.42) | copy-start | bytes 6148
  94.9 26.9 %copy-start.9 = (f32[1,512]{1,0:T(1,128)S(1)}, f32[1,512]{1,0:T(1,128)}, u32[]{:S(2)}) copy-start(f32[1,512]{1,0:T(1,128)} %get-tuple-element.43) | copy-start | bytes 6148
  94.9 26.9 %copy-start.10 = (f32[1,512]{1,0:T(1,128)S(1)}, f32[1,512]{1,0:T(1,128)}, u32[]{:S(2)}) copy-start(f32[1,512]{1,0:T(1,128)} %get-tuple-element.44) | copy-start | bytes 6148
  94.9 26.9 %copy-start.11 = (f32[1,512]{1,0:T(1,128)S(1)}, f32[1,512]{1,0:T(1,128)}, u32[]{:S(2)}) copy-start(f32[1,512]{1,0:T(1,128)} %get-tuple-element.45) | copy-start | bytes 6148
  95.0 26.9 %copy-start.12 = (f32[1,512]{1,0:T(1,128)S(1)}, f32[1,512]{1,0:T(1,128)}, u32[]{:S(2)}) copy-start(f32[1,512]{1,0:T(1,128)} %get-tuple-element.46) | copy-start | bytes 6148
  95.0 26.9 %copy-start.13 = (f32[1,512]{1,0:T(1,128)S(1)}, f32[1,512]{1,0:T(1,128)}, u32[]{:S(2)}) copy-start(f32[1,512]{1,0:T(1,128)} %get-tuple-element.47) | copy-start | bytes 6148
  95.0 26.9 %copy-start.14 = (f32[1,512]{1,0:T(1,128)S(1)}, f32[1,512]{1,0:T(1,128)}, u32[]{:S(2)}) copy-start(f32[1,512]{1,0:T(1,128)} %get-tuple-element.48) | copy-start | bytes 6148
  95.0 26.9 %copy-start.15 = (f32[1,512]{1,0:T(1,128)S(1)}, f32[1,512]{1,0:T(1,128)}, u32[]{:S(2)}) copy-start(f32[1,512]{1,0:T(1,128)} %get-tuple-element.49) | copy-start | bytes 6148
  95.0 26.9 %copy-start.16 = (f32[1,512]{1,0:T(1,128)S(1)}, f32[1,512]{1,0:T(1,128)}, u32[]{:S(2)}) copy-start(f32[1,512]{1,0:T(1,128)} %get-tuple-element.50) | copy-start | bytes 6148
  95.0 26.9 %copy-start.17 = (f32[1,512]{1,0:T(1,128)S(1)}, f32[1,512]{1,0:T(1,128)}, u32[]{:S(2)}) copy-start(f32[1,512]{1,0:T(1,128)} %get-tuple-element.51) | copy-start | bytes 6148
  121.9 9.1 %copy-start.18 = (f32[512]{0:T(512)S(1)}, f32[512]{0:T(512)}, u32[]{:S(2)}) copy-start(f32[512]{0:T(512)} %param.26) | copy-start | bytes 6148
  121.9 9.1 %copy-start.19 = (f32[512]{0:T(512)S(1)}, f32[512]{0:T(512)}, u32[]{:S(2)}) copy-start(f32[512]{0:T(512)} %param.25) | copy-start | bytes 6148
  161.6 2.5 %copy-start.6 = (f32[4,2,512]{2,1,0:T(2,128)S(1)}, f32[4,2,512]{2,1,0:T(2,128)}, u32[]{:S(2)}) copy-start(f32[4,2,512]{2,1,0:T(2,128)} %get-tuple-element.15) | copy-start | bytes 49156

commit v3 on v2

--- a/solution.py
+++ b/solution.py
@@ -163,13 +163,12 @@
     )(q, kv)
 
 
-def collect_kernel(ways, group, tp, att_ref, lt_ref, conv_ref, ao_ref, lo_ref, co_ref, asend, arecv, lsend, lrecv, csend, crecv, local):
+def collect_kernel(ways, group, tp, att_ref, lt_ref, ao_ref, lo_ref, asend, arecv, lsend, lrecv, local):
     me = lax.axis_index("sp")
     t = lax.axis_index("tp")
     a = me // group
     g = me % group
     vdim = att_ref.shape[-1]
-    cch = conv_ref.shape[-1]
 
     def coords(i):
         dt, da = i % tp, i // tp
@@ -189,10 +188,13 @@
 
     head = t * ways + a
 
+    def lanes(slot):
+        return ao_ref.at[:, pl.ds(pl.multiple_of(slot * vdim, 128), vdim)]
+
     def att_copy(i, slot):
         pa, pt = coords(i)
         return pltpu.make_async_remote_copy(
-            src_ref=att_ref.at[pa, pt], dst_ref=ao_ref.at[slot], send_sem=asend.at[i], recv_sem=arecv.at[slot],
+            src_ref=att_ref.at[pa, pt], dst_ref=lanes(slot), send_sem=asend.at[i], recv_sem=arecv.at[slot],
             device_id={"sp": pa * group + flipped(g, pa, group), "tp": pt}, device_id_type=MESH)
 
     def lt_copy(i, slot):
@@ -207,22 +209,12 @@
         c = att_copy(i, head)
         c.start()
         sends.append(c)
-    for i in range(1, tp):
-        pa, pt = coords(i)
-        c = pltpu.make_async_remote_copy(
-            src_ref=conv_ref.at[pt], dst_ref=co_ref.at[t],
-            send_sem=csend.at[i], recv_sem=crecv.at[t],
-            device_id={"sp": me, "tp": pt}, device_id_type=MESH)
-        c.start()
-        sends.append(c)
     for i in range(1, ways):
         c = lt_copy(i, a)
         c.start()
         sends.append(c)
-    keep = pltpu.make_async_copy(conv_ref.at[t], co_ref.at[t], local.at[1])
-    keep.start()
     mine = [
-        pltpu.make_async_copy(att_ref.at[a, t], ao_ref.at[head], local.at[0]),
+        pltpu.make_async_copy(att_ref.at[a, t], lanes(head), local.at[0]),
         pltpu.make_async_copy(lt_ref.at[a], lo_ref.at[a], local.at[2]),
     ]
 
@@ -239,17 +231,10 @@
     for i in range(1, total):
         pa, pt = coords(i)
         att_copy(i, pt * ways + pa).wait_recv()
-    for i in range(1, tp):
-        pa, pt = coords(i)
-        pltpu.make_async_remote_copy(
-            src_ref=conv_ref.at[t], dst_ref=co_ref.at[pt],
-            send_sem=csend.at[i], recv_sem=crecv.at[pt],
-            device_id={"sp": me, "tp": pt}, device_id_type=MESH).wait_recv()
     for i in range(1, ways):
         lt_copy(i, lax.rem(a + i, ways)).wait_recv()
     for c in sends:
         c.wait_send()
-    keep.wait()
 
     @pl.when(stays)
     def _():
@@ -263,31 +248,29 @@
             lt_copy(0, a).wait()
 
 
-def collect(att, lt, conv, ways, group, tp):
+def collect(att, lt, ways, group, tp):
     any_ = pl.BlockSpec(memory_space=pl.ANY)
     rows, vdim = att.shape[2:]
     total = ways * tp
     return pl.pallas_call(
         lambda *refs: collect_kernel(ways, group, tp, *refs),
         out_shape=(
-            jax.ShapeDtypeStruct((total, rows, vdim), att.dtype),
+            jax.ShapeDtypeStruct((rows, total * vdim), att.dtype),
             jax.ShapeDtypeStruct(lt.shape, lt.dtype),
-            jax.ShapeDtypeStruct(conv.shape, conv.dtype),
         ),
-        in_specs=[any_] * 3,
-        out_specs=(any_,) * 3,
+        in_specs=[any_] * 2,
+        out_specs=(any_,) * 2,
         scratch_shapes=[
             pltpu.SemaphoreType.DMA((total,)),
             pltpu.SemaphoreType.DMA((total,)),
             pltpu.SemaphoreType.DMA((ways,)),
             pltpu.SemaphoreType.DMA((ways,)),
-            pltpu.SemaphoreType.DMA((tp,)),
-            pltpu.SemaphoreType.DMA((tp,)),
             pltpu.SemaphoreType.DMA((3,)),
         ],
         compiler_params=pltpu.CompilerParams(collective_id=2, has_side_effects=True),
+        cost_estimate=pl.CostEstimate(flops=0, bytes_accessed=32 * att.size, transcendentals=0),
         name="collect",
-    )(att, lt, conv)
+    )(att, lt)
 
 
 def attention(place, lam, head_gain, qt, kv, tile=512):
@@ -349,7 +332,10 @@
         in_specs=[smem, smem, pl.BlockSpec((vdim, 1), lambda i, s: (0, 0)), pl.BlockSpec((1, qdim, tile), lambda i, s: (i, 0, s)), pl.BlockSpec(kv.shape, lambda i, s: (0, 0, 0))],
         out_specs=(pl.BlockSpec((1, tile, vdim), lambda i, s: (i, s, 0)), pl.BlockSpec((1, 2, tile), lambda i, s: (i, 0, s))),
         scratch_shapes=[pltpu.VMEM((2,rows,tile),jnp.float32),pltpu.VMEM((2,rows,tile),jnp.float32),pltpu.VMEM((2,vdim+16,tile),jnp.float32)],
-        compiler_params=pltpu.CompilerParams(vmem_limit_bytes=58 << 20), name="attend")(place, lam, head_gain.reshape(-1, 1), qt, kv)
+        compiler_params=pltpu.CompilerParams(vmem_limit_bytes=40 << 20), name="attend",
+        cost_estimate=pl.CostEstimate(
+            flops=blocks * rows * ways * rows * 6 * vdim, bytes_accessed=2 * kv.size,
+            transcendentals=blocks * rows * ways * rows))(place, lam, head_gain.reshape(-1, 1), qt, kv)
 
 
 def prepare_t(raw, qk_gain, cosine, sine):
@@ -438,12 +424,20 @@
     place = (me % group).astype(jnp.int32).reshape(1)
     lam = lax.dynamic_slice(mix_lambda, (me // group,), (1,))
     att, lt = attention(place, lam, head_gain, qall, kvall)
-    ao, lo, co = collect(
-        att.reshape(ways, tp, own, value_size), lt, conv_out.reshape(tp, own, conv_here), ways, group, tp)
-    heads = ways * tp
-    merged = jnp.concatenate([
-        jnp.transpose(ao, (1, 0, 2)).reshape(own, heads * value_size),
-        jnp.transpose(co, (1, 0, 2)).reshape(own, channels)], axis=1)
+    pieces = conv_out.reshape(tp, own, conv_here)
+    got = [lax.dynamic_index_in_dim(pieces, t, 0, keepdims=False)]
+    for d in range(1, tp):
+        piece = lax.dynamic_index_in_dim(pieces, (t + d) % tp, 0, keepdims=False)
+        got.append(lax.ppermute(piece, "tp", [(i, (i + d) % tp) for i in range(tp)]))
+    if tp == 2:
+        first = jnp.where(t == 0, got[0], got[1])
+        second = jnp.where(t == 0, got[1], got[0])
+        co = [first, second]
+    else:
+        stack = jnp.stack(got)
+        co = [lax.dynamic_index_in_dim(stack, (t - j) % tp, 0, keepdims=False) for j in range(tp)]
+    ao, lo = collect(att.reshape(ways, tp, own, value_size), lt, ways, group, tp)
+    merged = jnp.concatenate([ao] + co, axis=1)
     mixed = jnp.dot(merged, output_weight, preferred_element_type=jnp.float32).astype(jnp.bfloat16)
     return (mixed, jnp.transpose(lo, (1, 0, 2)))
 

time: 172 us -> 174 us (1.012)
  the two profiles are of different devices: /device:TPU:11 before, /device:TPU:1 now
where the time goes in v3:
time: 174 us
  Pallas kernels  91.3 us (52%)
  local copies, waits for them, and re-layouts  19.1 us (11%)
  waiting for transfers between devices  16.7 us (10%)
  matrix products  16.7 us (10%)
  other arithmetic  16.1 us (9%)
  starting transfers between devices  8.15 us (5%)
  blocking collectives  4.11 us (2%)
    pallas_call x1, Pallas kernels, spread(): pl.pallas_call(lambda *refs: spread_kernel(ways, group, *refs), out_shape...  40.7 us
    pallas_call x1, Pallas kernels, collect(): pl.pallas_call(lambda *refs: collect_kernel(ways, group, tp, *refs), out_...  27.2 us
    pallas_call x1, Pallas kernels, attention(): pl.pallas_call(kernel, grid=(ways, tiles), out_shape=(jax.ShapeDtypeStruc...  23.5 us
    ppermute x1, waiting for transfers between devices, per_device(): lax.ppermute(tokens, 'tp', [(i, (i - d) % tp) for i in range(tp)])  16.7 us
    unnamed x93, local copies, waits for them, and re-layouts  7.05 us
    dot_general x1, matrix products, per_device(): jnp.dot(merged, output_weight, preferred_element_type=jnp.float32)  6.87 us
    reduce_sum x1, other arithmetic, per_device(): jnp.sum(convolved, axis=1)  5.76 us
    dot_general x3, matrix products, turned(): lax.dot_general(matrix, normed, (((0,), (1,)), ((), ())), preferred_eleme...  4.99 us
  transfers between devices with their start and end apart: 3, of which 1 were waited for; matrix products, arithmetic and copies ran while one was open for 9% of the time, Pallas kernels for 53%

profile of v3, /device:TPU:1, one launch (start us, length us, event | category | flops | bytes accessed | tf_op | source)
XLA Modules:
  0.0 173.5 jit_solution(11235599150444680325)
XLA Ops:
  0.6 0.0 copy-start
  0.6 2.1 %collective-permute-start = (bf16[256,2048]{1,0:T(8,128)(2,1)}, bf16[256,2048]{1,0:T(8,128)(2,1)}, u32[]{:S(2)}, u32[]{:S(2)}) collective-permute-start(bf16[256,2048]{1,0:T(8,128)(2,1)} %param.14), channel_id=1, source_target_pairs={{0,1},{1,0},{2,3},{3,2},{4,5},{5,4},{6,7},{7,6},{8,9},{9,8},{10,11... | collective-permute-start | bytes 3145736 | tf_op jit(solution)/shard_map/ppermute | solution.py:378
  2.7 0.8 copy.24.gain_ref
  3.5 1.3 dynamic_slice.10.lam_ref
  4.8 1.6 fusion.58
  6.5 1.8 %fusion.57 = (f32[1,512]{1,0:T(1,128)}, f32[1,512]{1,0:T(1,128)}, f32[1,512]{1,0:T(1,128)}, f32[1,512]{1,0:T(1,128)}, f32[1,512]{1,0:T(1,128)}, /*index=5*/f32[1...) fusion(f32[31,512]{1,0:T(8,128)} %param.24), kind=kLoop, calls=%fused_computation.119 | loop fusion | bytes 77824 | tf_op jit(solution)/shard_map/slice | solution.py:413
  8.2 0.9 multiply_cosine_fusion
  9.2 16.7 %collective-permute-done = bf16[256,2048]{1,0:T(8,128)(2,1)} collective-permute-done((bf16[256,2048]{1,0:T(8,128)(2,1)}, bf16[256,2048]{1,0:T(8,128)(2,1)}, u32[]{:S(2)}, u32[]{:S(2)}) %collective-permute-start) | collective-permute-done | bytes 1048608 | tf_op jit(solution)/shard_map/ppermute | solution.py:378
  25.9 1.7 broadcast_select_fusion.1
  27.6 0.0 copy-start.5
  27.6 0.0 copy-start.42
  27.6 0.0 copy-start.45
  27.6 0.5 fusion
  28.1 0.4 copy-done.5
  28.6 1.0 copy-done.42
  29.6 2.1 %fusion.13 = bf16[512,512]{0,1:T(8,128)(2,1)} fusion(bf16[2048,512]{1,0:T(8,128)(2,1)S(1)} %copy-done.42, f32[2048]{0:T(1024)S(1)} %copy-done.45, f32[512]{0:T(512)S(1)} %add_rsqrt_fusion.3, bf16[256,2048]{1,0:T(8,128)(2,1)S(1)} %get-tuple-element.24, bf16[256,2048]{1,0:T(8,128)(2,1)S(1)} %get-tuple-element.23), kind=kOutput, calls=%fused_computation.22 | convolution fusion | flops 1081344000 | bytes 4728832 | tf_op jit(solution)/shard_map/dot_general | solution.py:389
  31.7 2.0 %reshape_reshape.3 = bf16[4,128,4,128]{1,0,3,2:T(4,128)(2,1)} reshape(bf16[512,512]{0,1:T(8,128)(2,1)} %fusion.13) | data formatting | bytes 1048576 | tf_op jit(solution)/shard_map/reshape;reshape | solution.py:404
  33.7 2.1 %copy.23 = bf16[4,128,4,128]{3,1,2,0:T(8,128)(2,1)} copy(bf16[4,128,4,128]{1,0,3,2:T(4,128)(2,1)} %reshape_reshape.3) | data formatting | bytes 1048576 | tf_op jit(solution)/shard_map/reshape;reshape | solution.py:404
  35.8 3.5 %fusion.7 = f32[512,512]{1,0:T(8,128)S(1)} fusion(bf16[2048,512]{1,0:T(8,128)(2,1)} %param.20, f32[2048]{0:T(1024)S(1)} %copy-done.45, f32[512]{0:T(512)S(1)} %add_rsqrt_fusion.3, bf16[256,2048]{1,0:T(8,128)(2,1)} %copy-done.5, bf16[256,2048]{1,0:T(8,128)(2,1)S(1)} %get-tuple-element.23), kind=kOutput, calls=%fused_computation.12 | convolution fusion | flops 1082392576 | bytes 5253120 | tf_op jit(solution)/shard_map/dot_general | solution.py:392
  39.3 1.3 fusion.12
  40.7 0.7 slice.272
  41.3 0.1 copy-done.9
  41.5 4.8 %collective-permute-start.1 = (bf16[30,512]{1,0:T(8,128)(2,1)}, bf16[30,512]{1,0:T(8,128)(2,1)}, u32[]{:S(2)}, u32[]{:S(2)}) collective-permute-start(bf16[30,512]{1,0:T(8,128)(2,1)} %slice.272), channel_id=1, source_target_pairs={{0,2},{2,4},{4,6},{6,8},{8,10},{10,12},{12,14},{14,16},{16,18},{18... | collective-permute-start | bytes 92168 | tf_op jit(solution)/shard_map/ppermute | solution.py:17
  46.3 1.4 multiply_reduce_fusion.1
  47.8 0.0 copy-start.41
  47.8 1.5 multiply_reduce_fusion.2
  49.3 0.5 multiply_multiply_fusion
  49.8 0.4 copy-done.11
  50.1 1.1 subtract_convert_fusion
  51.3 1.0 copy.22
  52.3 2.1 %pad_maximum_fusion.1.refs_1_ = bf16[4,1024,128]{2,1,0:T(8,128)(2,1)} fusion(bf16[4,512,128]{2,1,0:T(8,128)(2,1)S(1)} %bitcast.72, bf16[4,512,128]{2,1,0:T(8,128)(2,1)} %bitcast.73), kind=kLoop, calls=%fused_computation.84 | loop fusion | flops 2097152 | bytes 2097152 | tf_op jit(solution)/shard_map/concatenate | solution.py:404
  54.7 0.9 maximum_multiply_fusion
  55.6 40.7 %spread.1 = (bf16[4,128,512]{2,1,0:T(8,128)(2,1)}, bf16[16,1024,128]{2,1,0:T(8,128)(2,1)}) custom-call(bf16[4,128,512]{2,1,0:T(8,128)(2,1)} %bitcast.70, bf16[4,1024,128]{2,1,0:T(8,128)(2,1)} %pad_maximum_fusion.1.refs_1_), custom_call_target="tpu_custom_call" | custom-call | tf_op jit(solution)/shard_map/spread/pallas_call | solution.py:144
  96.3 0.9 maximum_convert_fusion
  97.5 0.0 copy-start.39
  97.5 0.0 copy-start.40
  97.5 5.8 %fusion.55 = (f32[512]{0:T(512)S(1)}, f32[512]{0:T(512)S(1)}, f32[512,512]{1,0:T(8,128)}) fusion(f32[542,512]{1,0:T(8,128)S(1)} %maximum_convert_fusion, f32[512]{0:T(512)S(1)} %bitcast.85, f32[512]{0:T(512)S(1)} %bitcast.86, f32[512]{0:T(512)S(1)} %bitcast.88, f32[512]{0:T(512)S(1)} %bitcast.89, f32[512]{0:T(512)S(1)} %bitcast.90, f32[512]{0:T(512)S(1)} %bitcast.91, ...), kind=kLoop, calls=%fused_computation.118 | loop fusion | flops 16776192 | bytes 33622016 | tf_op jit(solution)/shard_map/reduce_sum | solution.py:415
  103.2 4.1 %all-reduce = (f32[512]{0:T(512)S(1)}, f32[512]{0:T(512)S(1)}) all-reduce(f32[512]{0:T(512)S(1)} %get-tuple-element.19, f32[512]{0:T(512)S(1)} %get-tuple-element.18), channel_id=1, replica_groups=mesh['sp'=16,'tp'=2] {'tp'}, use_global_device_ids=true, to_apply=%region_6.7 | all-reduce | flops 1024 | bytes 8192 | tf_op jit(solution)/shard_map/psum | solution.py:414
  107.4 1.6 multiply_convert_fusion
  109.0 0.7 dynamic-slice_bitcast_fusion
  109.8 1.2 collective-permute-start.2
  111.0 2.2 %copy-done.3 = bf16[16,1024,128]{2,1,0:T(8,128)(2,1)S(1)} copy-done((bf16[16,1024,128]{2,1,0:T(8,128)(2,1)S(1)}, bf16[16,1024,128]{2,1,0:T(8,128)(2,1)}, u32[]{:S(2)}) %copy-start.3) | copy-done | bytes 4194328
  113.2 23.5 %attend.1 = (bf16[4,512,128]{2,1,0:T(8,128)(2,1)S(1)}, f32[4,2,512]{2,1,0:T(2,128)S(1)}) custom-call(s32[1]{0:T(128)} %bitcast.place_ref, f32[1]{0:T(128)} %dynamic_slice.10.lam_ref, f32[128,1]{1,0:T(8,128)S(1)} %copy.24.gain_ref, bf16[4,128,512]{2,1,0:T(8,128)(2,1)S(1)} %copy-done.4, bf16[16,1024,128]{2,1,0:T(8,128)(2,1)S(1)} %copy-done.3), custom_call_target="tpu_custom_call" | custom-call | flops 12884901888 | bytes 4194304 | tf_op jit(solution)/shard_map/attend/pallas_call | solution.py:330
  136.7 0.8 copy-done.1
  137.5 0.6 copy-done.2
  138.1 27.2 %collect.1 = (bf16[256,1024]{1,0:T(8,128)(2,1)}, f32[4,2,512]{2,1,0:T(2,128)}) custom-call(bf16[4,2,256,128]{3,2,1,0:T(8,128)(2,1)} %bitcast.67, f32[4,2,512]{2,1,0:T(2,128)} %copy-done.2), custom_call_target="tpu_custom_call" | custom-call | bytes 8388608 | tf_op jit(solution)/shard_map/collect/pallas_call | solution.py:255
  165.3 1.3 copy.25
  166.6 6.9 %convolution_convert_fusion = bf16[256,2048]{1,0:T(8,128)(2,1)} fusion(bf16[2048,2048]{1,0:T(8,128)(2,1)} %param.27, bf16[256,512]{1,0:T(8,128)(2,1)S(1)} %get-tuple-element.30, bf16[256,512]{1,0:T(8,128)(2,1)S(1)} %get-tuple-element.29, bf16[256,1024]{1,0:T(8,128)(2,1)} %get-tuple-element.12), kind=kOutput, calls=%fused_computation.5 | convolution fusion | flops 2151153664 | bytes 10485760 | tf_op jit(solution)/shard_map/dot_general | solution.py:441
  (87 shorter events, 0.3 us)
Async XLA Ops:
  0.6 45.7 %copy-start = (bf16[2048,512]{1,0:T(8,128)(2,1)S(1)}, bf16[2048,512]{1,0:T(8,128)(2,1)}, u32[]{:S(2)}) copy-start(bf16[2048,512]{1,0:T(8,128)(2,1)} %param.17) | copy-start | bytes 6291460
  0.6 25.3 %collective-permute-start = (bf16[256,2048]{1,0:T(8,128)(2,1)}, bf16[256,2048]{1,0:T(8,128)(2,1)}, u32[]{:S(2)}, u32[]{:S(2)}) collective-permute-start(bf16[256,2048]{1,0:T(8,128)(2,1)} %param.14), channel_id=1, source_target_pairs={{0,1},{1,0},{2,3},{3,2},{4,5},{5,4},{6,7},{7,6},{8,9},{9,8},{10,11... | collective-permute-start | bytes 3145736 | tf_op jit(solution)/shard_map/ppermute | solution.py:378
  27.6 1.0 copy-start.5
  27.6 2.0 %copy-start.42 = (bf16[2048,512]{1,0:T(8,128)(2,1)S(1)}, bf16[2048,512]{1,0:T(8,128)(2,1)}, u32[]{:S(2)}) copy-start(bf16[2048,512]{1,0:T(8,128)(2,1)} %param.18) | copy-start | bytes 6291460
  27.6 2.0 %copy-start.45 = (f32[2048]{0:T(1024)S(1)}, f32[2048]{0:T(1024)}, u32[]{:S(2)}) copy-start(f32[2048]{0:T(1024)} %param.15) | copy-start | bytes 24580
  35.8 3.5 %copy-start.6 = (bf16[256,2048]{1,0:T(8,128)(2,1)S(1)}, bf16[256,2048]{1,0:T(8,128)(2,1)}, u32[]{:S(2)}) copy-start(bf16[256,2048]{1,0:T(8,128)(2,1)} %copy-done.5) | copy-start | bytes 3145732
  35.8 3.5 %copy-start.43 = (bf16[2048,512]{1,0:T(8,128)(2,1)S(1)}, bf16[2048,512]{1,0:T(8,128)(2,1)}, u32[]{:S(2)}) copy-start(bf16[2048,512]{1,0:T(8,128)(2,1)} %param.19) | copy-start | bytes 6291460
  40.6 0.8 copy-start.9
  41.5 6.3 %copy-start.44 = (bf16[2048,512]{1,0:T(8,128)(2,1)S(1)}, bf16[2048,512]{1,0:T(8,128)(2,1)}, u32[]{:S(2)}) copy-start(bf16[2048,512]{1,0:T(8,128)(2,1)} %param.16) | copy-start | bytes 6291460
  41.5 54.8 %collective-permute-start.1 = (bf16[30,512]{1,0:T(8,128)(2,1)}, bf16[30,512]{1,0:T(8,128)(2,1)}, u32[]{:S(2)}, u32[]{:S(2)}) collective-permute-start(bf16[30,512]{1,0:T(8,128)(2,1)} %slice.272), channel_id=1, source_target_pairs={{0,2},{2,4},{4,6},{6,8},{8,10},{10,12},{12,14},{14,16},{16,18},{18... | collective-permute-start | bytes 92168 | tf_op jit(solution)/shard_map/ppermute | solution.py:17
  47.8 1.5 copy-start.41
  49.3 0.8 copy-start.11
  50.1 2.1 %copy-start.7 = (bf16[4,128,4,128]{3,1,2,0:T(8,128)(2,1)S(1)}, bf16[4,128,4,128]{3,1,2,0:T(8,128)(2,1)}, u32[]{:S(2)}) copy-start(bf16[4,128,4,128]{3,1,2,0:T(8,128)(2,1)} %copy.23) | copy-start | bytes 1572868
  52.3 2.1 %copy-start.8 = (bf16[4,2,32,512]{3,2,1,0:T(8,128)(2,1)S(1)}, bf16[4,2,32,512]{3,2,1,0:T(8,128)(2,1)}, u32[]{:S(2)}) copy-start(bf16[4,2,32,512]{3,2,1,0:T(8,128)(2,1)} %get-tuple-element.32) | copy-start | bytes 786436
  54.4 41.8 %copy-start.10 = (bf16[512,512]{1,0:T(8,128)(2,1)S(1)}, bf16[512,512]{1,0:T(8,128)(2,1)}, u32[]{:S(2)}) copy-start(bf16[512,512]{1,0:T(8,128)(2,1)} %copy-done.9) | copy-start | bytes 1572868
  54.4 42.8 %copy-start.12 = (f32[1,512]{1,0:T(1,128)S(1)}, f32[1,512]{1,0:T(1,128)}, u32[]{:S(2)}) copy-start(f32[1,512]{1,0:T(1,128)} %get-tuple-element.56) | copy-start | bytes 6148
  54.4 42.8 %copy-start.13 = (f32[1,512]{1,0:T(1,128)S(1)}, f32[1,512]{1,0:T(1,128)}, u32[]{:S(2)}) copy-start(f32[1,512]{1,0:T(1,128)} %get-tuple-element.57) | copy-start | bytes 6148
  54.4 42.8 %copy-start.14 = (f32[1,512]{1,0:T(1,128)S(1)}, f32[1,512]{1,0:T(1,128)}, u32[]{:S(2)}) copy-start(f32[1,512]{1,0:T(1,128)} %get-tuple-element.58) | copy-start | bytes 6148
  54.4 42.8 %copy-start.15 = (f32[1,512]{1,0:T(1,128)S(1)}, f32[1,512]{1,0:T(1,128)}, u32[]{:S(2)}) copy-start(f32[1,512]{1,0:T(1,128)} %get-tuple-element.59) | copy-start | bytes 6148
  54.5 42.8 %copy-start.16 = (f32[1,512]{1,0:T(1,128)S(1)}, f32[1,512]{1,0:T(1,128)}, u32[]{:S(2)}) copy-start(f32[1,512]{1,0:T(1,128)} %get-tuple-element.60) | copy-start | bytes 6148
  54.5 42.8 %copy-start.17 = (f32[1,512]{1,0:T(1,128)S(1)}, f32[1,512]{1,0:T(1,128)}, u32[]{:S(2)}) copy-start(f32[1,512]{1,0:T(1,128)} %get-tuple-element.61) | copy-start | bytes 6148
  54.5 42.8 %copy-start.18 = (f32[1,512]{1,0:T(1,128)S(1)}, f32[1,512]{1,0:T(1,128)}, u32[]{:S(2)}) copy-start(f32[1,512]{1,0:T(1,128)} %get-tuple-element.62) | copy-start | bytes 6148
  54.5 42.8 %copy-start.19 = (f32[1,512]{1,0:T(1,128)S(1)}, f32[1,512]{1,0:T(1,128)}, u32[]{:S(2)}) copy-start(f32[1,512]{1,0:T(1,128)} %get-tuple-element.63) | copy-start | bytes 6148
  54.5 42.8 %copy-start.20 = (f32[1,512]{1,0:T(1,128)S(1)}, f32[1,512]{1,0:T(1,128)}, u32[]{:S(2)}) copy-start(f32[1,512]{1,0:T(1,128)} %get-tuple-element.33) | copy-start | bytes 6148
  54.5 42.8 %copy-start.21 = (f32[1,512]{1,0:T(1,128)S(1)}, f32[1,512]{1,0:T(1,128)}, u32[]{:S(2)}) copy-start(f32[1,512]{1,0:T(1,128)} %get-tuple-element.34) | copy-start | bytes 6148
  54.5 42.8 %copy-start.22 = (f32[1,512]{1,0:T(1,128)S(1)}, f32[1,512]{1,0:T(1,128)}, u32[]{:S(2)}) copy-start(f32[1,512]{1,0:T(1,128)} %get-tuple-element.35) | copy-start | bytes 6148
  54.5 42.8 %copy-start.23 = (f32[1,512]{1,0:T(1,128)S(1)}, f32[1,512]{1,0:T(1,128)}, u32[]{:S(2)}) copy-start(f32[1,512]{1,0:T(1,128)} %get-tuple-element.36) | copy-start | bytes 6148
  54.5 42.8 %copy-start.24 = (f32[1,512]{1,0:T(1,128)S(1)}, f32[1,512]{1,0:T(1,128)}, u32[]{:S(2)}) copy-start(f32[1,512]{1,0:T(1,128)} %get-tuple-element.37) | copy-start | bytes 6148
  54.5 42.8 %copy-start.25 = (f32[1,512]{1,0:T(1,128)S(1)}, f32[1,512]{1,0:T(1,128)}, u32[]{:S(2)}) copy-start(f32[1,512]{1,0:T(1,128)} %get-tuple-element.38) | copy-start | bytes 6148
  54.6 42.8 %copy-start.26 = (f32[1,512]{1,0:T(1,128)S(1)}, f32[1,512]{1,0:T(1,128)}, u32[]{:S(2)}) copy-start(f32[1,512]{1,0:T(1,128)} %get-tuple-element.39) | copy-start | bytes 6148
  54.6 42.8 %copy-start.27 = (f32[1,512]{1,0:T(1,128)S(1)}, f32[1,512]{1,0:T(1,128)}, u32[]{:S(2)}) copy-start(f32[1,512]{1,0:T(1,128)} %get-tuple-element.40) | copy-start | bytes 6148
  54.6 42.8 %copy-start.28 = (f32[1,512]{1,0:T(1,128)S(1)}, f32[1,512]{1,0:T(1,128)}, u32[]{:S(2)}) copy-start(f32[1,512]{1,0:T(1,128)} %get-tuple-element.41) | copy-start | bytes 6148
  54.6 42.8 %copy-start.29 = (f32[1,512]{1,0:T(1,128)S(1)}, f32[1,512]{1,0:T(1,128)}, u32[]{:S(2)}) copy-start(f32[1,512]{1,0:T(1,128)} %get-tuple-element.42) | copy-start | bytes 6148
  54.6 42.8 %copy-start.30 = (f32[1,512]{1,0:T(1,128)S(1)}, f32[1,512]{1,0:T(1,128)}, u32[]{:S(2)}) copy-start(f32[1,512]{1,0:T(1,128)} %get-tuple-element.43) | copy-start | bytes 6148
  54.6 42.8 %copy-start.31 = (f32[1,512]{1,0:T(1,128)S(1)}, f32[1,512]{1,0:T(1,128)}, u32[]{:S(2)}) copy-start(f32[1,512]{1,0:T(1,128)} %get-tuple-element.44) | copy-start | bytes 6148
  54.6 42.8 %copy-start.32 = (f32[1,512]{1,0:T(1,128)S(1)}, f32[1,512]{1,0:T(1,128)}, u32[]{:S(2)}) copy-start(f32[1,512]{1,0:T(1,128)} %get-tuple-element.45) | copy-start | bytes 6148
  54.6 42.8 %copy-start.33 = (f32[1,512]{1,0:T(1,128)S(1)}, f32[1,512]{1,0:T(1,128)}, u32[]{:S(2)}) copy-start(f32[1,512]{1,0:T(1,128)} %get-tuple-element.46) | copy-start | bytes 6148
  54.6 42.8 %copy-start.34 = (f32[1,512]{1,0:T(1,128)S(1)}, f32[1,512]{1,0:T(1,128)}, u32[]{:S(2)}) copy-start(f32[1,512]{1,0:T(1,128)} %get-tuple-element.47) | copy-start | bytes 6148
  54.6 42.8 %copy-start.35 = (f32[1,512]{1,0:T(1,128)S(1)}, f32[1,512]{1,0:T(1,128)}, u32[]{:S(2)}) copy-start(f32[1,512]{1,0:T(1,128)} %get-tuple-element.48) | copy-start | bytes 6148
  54.7 42.8 %copy-start.36 = (f32[1,512]{1,0:T(1,128)S(1)}, f32[1,512]{1,0:T(1,128)}, u32[]{:S(2)}) copy-start(f32[1,512]{1,0:T(1,128)} %get-tuple-element.49) | copy-start | bytes 6148
  54.7 42.8 %copy-start.37 = (f32[1,512]{1,0:T(1,128)S(1)}, f32[1,512]{1,0:T(1,128)}, u32[]{:S(2)}) copy-start(f32[1,512]{1,0:T(1,128)} %get-tuple-element.50) | copy-start | bytes 6148
  54.7 42.8 %copy-start.38 = (f32[1,512]{1,0:T(1,128)S(1)}, f32[1,512]{1,0:T(1,128)}, u32[]{:S(2)}) copy-start(f32[1,512]{1,0:T(1,128)} %get-tuple-element.51) | copy-start | bytes 6148
  97.5 9.9 %copy-start.39 = (f32[512]{0:T(512)S(1)}, f32[512]{0:T(512)}, u32[]{:S(2)}) copy-start(f32[512]{0:T(512)} %param.26) | copy-start | bytes 6148
  97.5 9.9 %copy-start.40 = (f32[512]{0:T(512)S(1)}, f32[512]{0:T(512)}, u32[]{:S(2)}) copy-start(f32[512]{0:T(512)} %param.25) | copy-start | bytes 6148
  103.2 7.8 %copy-start.4 = (bf16[4,128,512]{2,1,0:T(8,128)(2,1)S(1)}, bf16[4,128,512]{2,1,0:T(8,128)(2,1)}, u32[]{:S(2)}) copy-start(bf16[4,128,512]{2,1,0:T(8,128)(2,1)} %get-tuple-element.8.q_ref) | copy-start | bytes 1572868
  109.8 56.8 %collective-permute-start.2 = (bf16[256,512]{1,0:T(8,128)(2,1)}, bf16[256,512]{1,0:T(8,128)(2,1)S(1)}, u32[]{:S(2)}, u32[]{:S(2)}) collective-permute-start(bf16[256,512]{1,0:T(8,128)(2,1)} %dynamic-slice_bitcast_fusion), channel_id=1, source_target_pairs={{0,1},{1,0},{2,3},{3,2},{4,5},{5,4},{6,7},{7,6},{8,9},{9,8},{10,11... | collective-permute-start | bytes 786440 | tf_op jit(solution)/shard_map/ppermute | solution.py:431
  111.0 2.2 %copy-start.3 = (bf16[16,1024,128]{2,1,0:T(8,128)(2,1)S(1)}, bf16[16,1024,128]{2,1,0:T(8,128)(2,1)}, u32[]{:S(2)}) copy-start(bf16[16,1024,128]{2,1,0:T(8,128)(2,1)} %get-tuple-element.9.kv_ref) | copy-start | bytes 12582916
  136.7 0.8 copy-start.1
  (1 other events, 0.6 us)
